TPU v7x, 256 devices: a 4x2x16 block of a 4x16x16 slice. The times are simulated.
256 devices in a mesh: grp: 2 (over y), sp: 16 (over z), tp: 8 (over x, core).
Axes of the slice: x: 4, y: 2, z: 16, core: 2. Of those that a mesh axis runs over, the one named last changes fastest.
The devices are a block of a 4x16x16 slice.
Arguments:
- queries: bfloat16 [24576, 1024], P(('grp', 'sp'), 'tp'), parts along dimension 0, may hold values from -8 to 8
- keys: bfloat16 [24576, 256], P(('grp', 'sp')), parts along dimension 0, may hold values from -8 to 8
- values: bfloat16 [24576, 256], P(('grp', 'sp')), parts along dimension 0, may hold values from -6 to 6
- query_gain: float32 [128], replicated, may hold values from 0.2 to 6
- key_gain: float32 [128], replicated, may hold values from 0.2 to 6
- residual: bfloat16 [24576, 2048], P(('grp', 'sp', 'tp')), parts along dimension 0, may hold values from -6 to 6
- out_weight: bfloat16 [1024, 2048], P('tp'), may hold values from -0.1875 to 0.1875
- mix_gain: float32 [2048], replicated, may hold values from 0.1 to 1.9
- ffn_gain: float32 [2048], replicated, may hold values from 0.1 to 1.9
- gate_in: bfloat16 [2048, 5632], P('sp', 'tp'), may hold values from -0.125 to 0.125
- value_in: bfloat16 [2048, 5632], P('sp', 'tp'), may hold values from -0.125 to 0.125
- conv_gate: float32 [3, 5632], P(None, 'tp'), may hold values from -3 to 3
- conv_value: float32 [3, 5632], P(None, 'tp'), may hold values from -3 to 3
- down_t: bfloat16 [2048, 5632], P('sp', 'tp'), may hold values from -0.078125 to 0.078125
Outputs:
- layer_out: bfloat16 [24576, 2048], P(('grp', 'sp', 'tp')), parts along dimension 0
There are 2 independent parts, one for each index of `grp`. A program takes and returns all parts, laid end to end along the dimension named above; an argument that names none is the same for every part. Nothing has to cross between parts.
All inputs are finite; a program needn't handle non-finite values.
Results may differ from a plain program's by a relative error of at most 0.02.
The roundings to bfloat16 on the way count: a program that leaves them out, or rounds other values in their place, can miss the bound.
Values may be sent and summed in bfloat16 or wider, within the bound.
A program may use at most 128 MiB of HBM per device.

v0:
```python
import jax
import jax.numpy as jnp
from jax import lax
from jax.sharding import PartitionSpec as P

HEADS = 8
KVH = 2
GRID_W = 64


EPSILON = 1e-06
THETA = 10000.0


def sent_together(arrays, axis, dim, along):
    both = jnp.concatenate(arrays, axis=along)
    whole, at, gathered = (lax.all_gather(both, axis, axis=dim, tiled=True), 0, [])
    for a in arrays:
        gathered.append(lax.slice_in_dim(whole, at, at + a.shape[along], axis=along))
        at += a.shape[along]
    return tuple(gathered)


def cut_along(array, dim, size):
    before, after = (array.shape[:dim], array.shape[dim + 1 :])
    return jnp.moveaxis(array.reshape(*before, size, -1, *after), dim, 0)


def summed_on_arrival(array, axis, dim):
    tiles = cut_along(array, dim, lax.axis_size(axis))
    arrived = lax.all_to_all(tiles, axis, split_axis=0, concat_axis=0, tiled=True)
    return arrived.astype(jnp.float32).sum(axis=0)


def with_halo(block, sides, width):
    for axis, dim in sides:
        count = lax.axis_size(axis)
        forward = [(i, i + 1) for i in range(count - 1)]
        backward = [(target, source) for source, target in forward]
        low = lax.ppermute(
            lax.slice_in_dim(block, block.shape[dim] - width, None, axis=dim), axis, forward
        )
        high = lax.ppermute(lax.slice_in_dim(block, 0, width, axis=dim), axis, backward)
        block = jnp.concatenate([low, block, high], axis=dim)
    return block


def rotary_tables(positions, seq_total, head_dim):
    quarter = head_dim // 4
    inverse = THETA ** (-(2.0 * jnp.arange(quarter, dtype=jnp.float32)) / (head_dim // 2))
    grid_row = (positions // GRID_W - seq_total // GRID_W // 2).astype(jnp.float32)
    grid_col = (positions % GRID_W - GRID_W // 2).astype(jnp.float32)
    row_angle = grid_row[:, None] * inverse[None, :]
    col_angle = grid_col[:, None] * inverse[None, :]
    angle = jnp.concatenate([row_angle, row_angle, col_angle, col_angle], axis=-1)
    return (jnp.cos(angle), jnp.sin(angle))


def rotate_quarters(vector):
    first, second, third, fourth = jnp.split(vector, 4, axis=-1)
    return jnp.concatenate([-second, first, -fourth, third], axis=-1)


def prepare_heads(raw, gain, cos_table, sin_table, factor):
    floats = raw.astype(jnp.float32)
    normed = floats * lax.rsqrt(jnp.mean(floats * floats, axis=-1, keepdims=True) + EPSILON) * gain
    turned = normed * cos_table + rotate_quarters(normed) * sin_table
    return (turned * factor).astype(jnp.bfloat16)


def rms_rows(stream, gain):
    floats = stream.astype(jnp.float32)
    return floats * lax.rsqrt(jnp.mean(floats * floats, axis=-1, keepdims=True) + EPSILON) * gain


def body(
    queries,
    keys,
    values,
    query_gain,
    key_gain,
    residual,
    out_weight,
    mix_gain,
    ffn_gain,
    gate_in,
    value_in,
    conv_gate,
    conv_value,
    down_t,
):
    gate_rows, value_rows, down_rows = sent_together((gate_in, value_in, down_t), "sp", 0, 1)
    tok_rows = queries.shape[0]
    head_dim = query_gain.shape[0]
    local_heads = queries.shape[1] // head_dim
    seq_total = tok_rows * lax.axis_size("sp")
    kv_head = lax.axis_index("tp") * local_heads // (HEADS // KVH)
    positions = lax.axis_index("sp") * tok_rows + jnp.arange(tok_rows, dtype=jnp.int32)
    cos_table, sin_table = rotary_tables(positions, seq_total, head_dim)
    key_own = lax.dynamic_slice_in_dim(keys, kv_head * head_dim, head_dim, 1)
    value_own = lax.dynamic_slice_in_dim(values, kv_head * head_dim, head_dim, 1)
    key_rot = prepare_heads(key_own, key_gain, cos_table, sin_table, 1.0)
    query_rot = prepare_heads(
        queries.reshape(tok_rows, local_heads, head_dim),
        query_gain,
        cos_table[:, None, :],
        sin_table[:, None, :],
        head_dim ** (-0.5),
    )
    query_rows = jnp.transpose(query_rot, (1, 0, 2)).reshape(local_heads * tok_rows, head_dim)
    query_count = local_heads * tok_rows
    running = jnp.full((query_count, 1), -1e30, jnp.float32)
    key_piece, value_piece = sent_together((key_rot, value_own), "sp", 0, 1)
    scores = lax.dot_general(
        query_rows, key_piece, (((1,), (1,)), ((), ())), preferred_element_type=jnp.float32
    )
    newest = jnp.maximum(running, jnp.max(scores, axis=1, keepdims=True))
    weights = jnp.exp(scores - newest)
    denom = jnp.sum(weights, axis=1, keepdims=True)
    summed = jnp.dot(weights.astype(jnp.bfloat16), value_piece, preferred_element_type=jnp.float32)
    running, denom, summed = (newest, denom, summed)
    attended = (summed / denom).astype(jnp.bfloat16).reshape(local_heads, tok_rows, head_dim)
    attended = jnp.transpose(attended, (1, 0, 2)).reshape(tok_rows, local_heads * head_dim)
    block_rows = attended
    mix = summed_on_arrival(
        jnp.dot(block_rows, out_weight, preferred_element_type=jnp.float32).astype(jnp.bfloat16),
        "tp",
        0,
    )
    stream = (residual.astype(jnp.float32) + rms_rows(mix, mix_gain)).astype(jnp.bfloat16)
    normed = rms_rows(stream, ffn_gain).astype(jnp.bfloat16)
    paired = jnp.concatenate([gate_rows, value_rows], axis=1)
    upward = jnp.dot(
        lax.all_gather(normed, "tp", axis=0, tiled=True), paired, preferred_element_type=jnp.float32
    ).astype(jnp.bfloat16)
    padded = with_halo(upward, (("sp", 0),), 1).astype(jnp.float32)
    taps = jnp.concatenate([conv_gate, conv_value], axis=1)
    mixed = taps[0] * padded[:-2] + taps[1] * padded[1:-1] + taps[2] * padded[2:]
    unit_cols = conv_gate.shape[1]
    hidden = (jax.nn.gelu(mixed[:, :unit_cols], approximate=True) * mixed[:, unit_cols:]).astype(
        jnp.bfloat16
    )
    block_rows = hidden
    ffn_out = summed_on_arrival(
        lax.dot_general(
            block_rows, down_rows, (((1,), (1,)), ((), ())), preferred_element_type=jnp.float32
        ).astype(jnp.bfloat16),
        "tp",
        0,
    )
    return (stream.astype(jnp.float32) + ffn_out).astype(jnp.bfloat16)


def solution(mesh):
    return jax.shard_map(
        body,
        mesh=mesh,
        in_specs=(
            P(("grp", "sp"), "tp"),
            P(("grp", "sp"), None),
            P(("grp", "sp"), None),
            P(),
            P(),
            P(("grp", "sp", "tp"), None),
            P("tp", None),
            P(),
            P(),
            P("sp", "tp"),
            P("sp", "tp"),
            P(None, "tp"),
            P(None, "tp"),
            P("sp", "tp"),
        ),
        out_specs=P(("grp", "sp", "tp"), None),
        check_vma=False,
    )
```

profile of v0, /device:TPU:33, one launch (start us, length us, event | category | flops | bytes accessed | tf_op | source)
XLA Modules:
  0.0 345.3 jit_solution(11012669087130800998)
XLA Ops:
  6.5 0.0 copy-start
  6.6 0.0 copy-start.3
  6.6 0.0 copy-start.10
  6.6 0.0 all-gather.4.cloned.1.call-start
  6.6 1.2 fusion.55
  7.8 1.1 fusion.56
  8.9 0.0 copy-start.2
  8.9 0.0 copy-start.9
  8.9 0.4 slice_negate_fusion.1
  9.3 0.9 constant_dynamic-slice_fusion
  10.3 0.3 broadcast_multiply_fusion.1
  10.6 0.0 copy-done.3
  10.6 0.0 copy-done.10
  10.6 2.0 fusion.60
  12.6 0.8 pad_maximum_fusion.2
  13.4 0.1 all-gather.4.cloned.1.call-update
  13.4 0.1 all-gather.8.cloned.1.call-start
  13.5 1.9 pad_maximum_fusion
  15.4 0.1 all-gather.8.cloned.1.call-update
  15.5 0.1 all-gather.6.cloned.1.call-start
  15.6 0.0 copy-done.2
  15.6 0.2 fusion.48
  15.8 0.0 copy-done.9
  15.8 0.2 fusion.50
  16.0 0.4 fusion.58
  16.3 93.2 %all-gather.4.cloned.1.call-done = bf16[12288,256]{1,0:T(8,128)(2,1)} async-done(((bf16[768,256]{1,0:T(8,128)(2,1)}), bf16[12288,256]{1,0:T(8,128)(2,1)}) %all-gather.4.cloned.1.call-update) | async-done | bytes 6291472 | tf_op jit(solution)/shard_map/all_gather | solution.py:17
  109.5 16.3 %fusion.87 = (f32[768]{0:T(1024)S(1)}, f32[768,12288]{1,0:T(8,128)}) fusion(bf16[12288,256]{1,0:T(8,128)(2,1)} %all-gather.4.cloned.1.call-done, bf16[768,128]{1,0:T(8,128)(2,1)S(1)} %copy-done.2, f32[768,32]{1,0:T(8,128)S(1)} %get-tuple-element.13, f32[768,32]{1,0:T(8,128)S(1)} %get-tuple-element.14, f32[768,32]{1,0:T(8,128)S(1)} %get-tuple-element.15, ...), kind=kOutput, calls=%fused_computation.117 | convolution fusion | flops 2426731776 | bytes 41687552 | tf_op jit(solution)/shard_map/dot_general | solution.py:114
  125.9 15.4 %fusion = f32[768]{0:T(1024)S(1)} fusion(f32[768,12288]{1,0:T(8,128)} %get-tuple-element.23, f32[768]{0:T(1024)S(1)} %broadcast_maximum_fusion), kind=kLoop, calls=%fused_computation.1 | loop fusion | flops 18873600 | bytes 37754880 | tf_op jit(solution)/shard_map/reduce_sum | solution.py:119
  141.2 0.0 copy-done
  141.2 18.7 %convolution_convert_fusion.1 = bf16[768,2048]{1,0:T(8,128)(2,1)} fusion(bf16[128,2048]{1,0:T(8,128)(2,1)S(1)} %copy-done, bf16[12288,256]{1,0:T(8,128)(2,1)} %all-gather.4.cloned.1.call-done, f32[768,12288]{1,0:T(8,128)} %get-tuple-element.23, f32[768]{0:T(1024)S(1)} %broadcast_maximum_fusion, f32[768]{0:T(1024)S(1)} %fusion), kind=kOutput, calls=%fused_computation.16 | convolution fusion | flops 2839216128 | bytes 44570624 | tf_op jit(solution)/shard_map/dot_general | solution.py:126
  159.9 0.0 copy-start.4
  159.9 0.0 copy-start.7
  159.9 45.7 %all_to_all.10 = bf16[8,96,2048]{2,1,0:T(8,128)(2,1)S(1)} all-to-all(bf16[8,96,2048]{2,1,0:T(8,128)(2,1)} %bitcast.14), channel_id=1, replica_groups=mesh['grp'=2,'sp'=16,'tp'=8] {'tp'}, dimensions={0} | all-to-all | bytes 6291456 | tf_op jit(solution)/shard_map/all_to_all | solution.py:31
  205.6 0.0 copy-start.8
  205.6 0.6 convert_reduce_fusion.1
  206.2 0.1 multiply_reduce_fusion
  206.3 0.0 copy-done.4
  206.3 0.0 copy-done.7
  206.3 0.3 fusion.44
  206.7 0.0 copy-done.8
  206.7 0.9 fusion.46
  207.6 0.1 all-gather.6.cloned.1.call-update
  207.7 0.0 copy-start.5
  207.7 0.0 copy-start.6
  207.7 22.5 %all-gather.8.cloned.1.call-done = bf16[2048,2112]{0,1:T(8,128)(2,1)} async-done(((bf16[128,2112]{0,1:T(8,128)(2,1)}), bf16[2048,2112]{0,1:T(8,128)(2,1)}) %all-gather.8.cloned.1.call-update) | async-done | bytes 8650768 | tf_op jit(solution)/shard_map/all_gather | solution.py:17
  230.2 42.3 %all-gather.6.cloned.1.call-done = bf16[768,2048]{1,0:T(8,128)(2,1)} async-done(((bf16[96,2048]{1,0:T(8,128)(2,1)}), bf16[768,2048]{1,0:T(8,128)(2,1)}) %all-gather.6.cloned.1.call-update) | async-done | bytes 3145744 | tf_op jit(solution)/shard_map/all_gather | solution.py:134
  272.5 8.4 %fusion.9 = bf16[768,1408]{1,0:T(8,128)(2,1)S(1)} fusion(bf16[768,2048]{1,0:T(8,128)(2,1)} %all-gather.6.cloned.1.call-done, bf16[2048,2112]{0,1:T(8,128)(2,1)} %all-gather.8.cloned.1.call-done), kind=kOutput, calls=%fused_computation.17 | convolution fusion | flops 4430266368 | bytes 11075584 | tf_op jit(solution)/shard_map/dot_general | solution.py:133
  280.9 3.2 collective-permute-start
  284.1 1.3 collective-permute-start.1
  285.4 0.0 copy-done.5
  285.4 0.0 copy-done.6
  285.4 0.1 maximum_reduce_fusion.1
  285.5 0.0 collective-permute-done
  285.6 2.9 collective-permute-done.1
  288.5 0.4 maximum_convert_fusion
  288.9 1.3 fusion.7
  290.2 5.1 %convolution_convert_fusion = bf16[768,2048]{1,0:T(8,128)(2,1)S(1)} fusion(bf16[2048,2112]{0,1:T(8,128)(2,1)} %all-gather.8.cloned.1.call-done, f32[768,1408]{1,0:T(8,128)S(1)} %fusion.7), kind=kOutput, calls=%fused_computation.15 | convolution fusion | flops 2221572096 | bytes 10747904 | tf_op jit(solution)/shard_map/dot_general | solution.py:145
  295.3 0.0 copy-start.1
  295.3 42.0 %all_to_all.11 = bf16[8,96,2048]{2,1,0:T(8,128)(2,1)S(1)} all-to-all(bf16[8,96,2048]{2,1,0:T(8,128)(2,1)S(1)} %bitcast.15), channel_id=1, replica_groups=mesh['grp'=2,'sp'=16,'tp'=8] {'tp'}, dimensions={0} | all-to-all | bytes 6291456 | tf_op jit(solution)/shard_map/all_to_all | solution.py:31
  337.3 0.6 convert_reduce_fusion
  337.9 0.8 fusion.47
  338.7 0.0 copy-done.1
  (8 shorter events, 0.1 us)
Async XLA Ops:
  6.5 134.7 %copy-start = (bf16[128,2048]{1,0:T(8,128)(2,1)S(1)}, bf16[128,2048]{1,0:T(8,128)(2,1)}, u32[]{:S(2)}) copy-start(bf16[128,2048]{1,0:T(8,128)(2,1)} %param.20) | copy-start | bytes 1572868
  6.6 4.0 %copy-start.3 = (bf16[768,256]{1,0:T(8,128)(2,1)S(1)}, bf16[768,256]{1,0:T(8,128)(2,1)}, u32[]{:S(2)}) copy-start(bf16[768,256]{1,0:T(8,128)(2,1)} %param.15) | copy-start | bytes 1179652
  6.6 4.0 %copy-start.10 = (f32[128]{0:T(128)S(1)}, f32[128]{0:T(128)}, u32[]{:S(2)}) copy-start(f32[128]{0:T(128)} %param.18) | copy-start | bytes 1540
  6.6 103.0 %all-gather.4.cloned.1.call-start = ((), (), s32[]{:S(2)}) async-start(), calls=%async_computation.2 | async-start | bytes 6684672 | tf_op jit(solution)/shard_map/all_gather | solution.py:17
  8.9 6.6 %copy-start.2 = (bf16[768,128]{1,0:T(8,128)(2,1)S(1)}, bf16[768,128]{1,0:T(8,128)(2,1)}, u32[]{:S(2)}) copy-start(bf16[768,128]{1,0:T(8,128)(2,1)} %param.14) | copy-start | bytes 589828
  8.9 6.8 %copy-start.9 = (f32[128]{0:T(128)S(1)}, f32[128]{0:T(128)}, u32[]{:S(2)}) copy-start(f32[128]{0:T(128)} %param.17) | copy-start | bytes 1540
  13.4 216.8 %all-gather.8.cloned.1.call-start = ((), (), s32[]{:S(2)}) async-start(), calls=%async_computation.4 | async-start | bytes 9191424 | tf_op jit(solution)/shard_map/all_gather | solution.py:17
  15.5 257.0 %all-gather.6.cloned.1.call-start = ((), (), s32[]{:S(2)}) async-start(), calls=%async_computation.3 | async-start | bytes 3538944 | tf_op jit(solution)/shard_map/all_gather | solution.py:134
  159.9 46.4 %copy-start.4 = (bf16[96,2048]{1,0:T(8,128)(2,1)S(1)}, bf16[96,2048]{1,0:T(8,128)(2,1)}, u32[]{:S(2)}) copy-start(bf16[96,2048]{1,0:T(8,128)(2,1)} %param.19) | copy-start | bytes 1179652
  159.9 46.4 %copy-start.7 = (f32[2048]{0:T(1024)S(1)}, f32[2048]{0:T(1024)}, u32[]{:S(2)}) copy-start(f32[2048]{0:T(1024)} %param.21) | copy-start | bytes 24580
  205.6 1.1 copy-start.8
  207.7 77.8 %copy-start.5 = (f32[3,704]{1,0:T(4,128)S(1)}, f32[3,704]{1,0:T(4,128)}, u32[]{:S(2)}) copy-start(f32[3,704]{1,0:T(4,128)} %param.26) | copy-start | bytes 25348
  207.7 77.8 %copy-start.6 = (f32[3,704]{1,0:T(4,128)S(1)}, f32[3,704]{1,0:T(4,128)}, u32[]{:S(2)}) copy-start(f32[3,704]{1,0:T(4,128)} %param.25) | copy-start | bytes 25348
  280.9 4.6 %collective-permute-start = (bf16[1,1408]{1,0:T(2,128)(2,1)S(1)}, bf16[1,1408]{1,0:T(2,128)(2,1)S(1)}, u32[]{:S(2)}, u32[]{:S(2)}) collective-permute-start(bf16[1,1408]{1,0:T(2,128)(2,1)S(1)} %get-tuple-element.10), channel_id=1, source_target_pairs={{0,8},{8,16},{16,24},{24,32},{32,40},{40,48},{48,56},{56,64},{64,7... | collective-permute-start | bytes 8456 | tf_op jit(solution)/shard_map/ppermute | solution.py:40
  284.1 4.4 %collective-permute-start.1 = (bf16[1,1408]{1,0:T(2,128)(2,1)S(1)}, bf16[1,1408]{1,0:T(2,128)(2,1)S(1)}, u32[]{:S(2)}, u32[]{:S(2)}) collective-permute-start(bf16[1,1408]{1,0:T(2,128)(2,1)S(1)} %get-tuple-element.11), channel_id=1, source_target_pairs={{8,0},{16,8},{24,16},{32,24},{40,32},{48,40},{56,48},{64,56},{72,6... | collective-permute-start | bytes 8456 | tf_op jit(solution)/shard_map/ppermute | solution.py:43
  295.3 43.4 %copy-start.1 = (bf16[128,2048]{1,0:T(8,128)(2,1)S(1)}, bf16[128,2048]{1,0:T(8,128)(2,1)}, u32[]{:S(2)}) copy-start(bf16[128,2048]{1,0:T(8,128)(2,1)} %param.20) | copy-start | bytes 1572868
Sparse Core Ops, SparseCore 0:
  13.5 95.9 all-gather.3
  111.3 118.8 all-gather.7
  232.0 40.3 all-gather.5
where the time goes:
time: 346 us; the launch traced here: 345 us
  waiting for transfers between devices  161 us (47%)
  blocking collectives  87.7 us (25%)
  matrix products  48.5 us (14%)
  other arithmetic  28.9 us (8%)
  between operations  13.4 us (4%)
  starting transfers between devices  4.63 us (1%)
    all_gather x2, waiting for transfers between devices, sent_together(): lax.all_gather(both, axis, axis=dim, tiled=True)  116 us
    all_to_all x2, blocking collectives, summed_on_arrival(): lax.all_to_all(tiles, axis, split_axis=0, concat_axis=0, tiled=True)  87.7 us
    all_gather x1, waiting for transfers between devices, body(): lax.all_gather(normed, 'tp', axis=0, tiled=True)  42.3 us
    dot_general x1, matrix products, body(): jnp.dot(block_rows, out_weight, preferred_element_type=jnp.float32)  18.7 us
    dot_general x1, matrix products, body(): lax.dot_general(query_rows, key_piece, (((1,), (1,)), ((), ())), preferre...  16.3 us
    reduce_sum x1, other arithmetic, body(): denom = jnp.sum(weights, axis=1, keepdims=True)  15.4 us
    dot_general x1, matrix products, body(): jnp.dot(lax.all_gather(normed, 'tp', axis=0, tiled=True), paired, preferr...  8.42 us
  transfers between devices with their start and end apart: 5, of which 4 were waited for; matrix products, arithmetic and copies ran while one was open for 16% of the time, Pallas kernels for 0%

commit v1 on v0

v1 whole, which is shorter than its diff:
```python
import functools

import jax
import jax.numpy as jnp
import numpy as np
from jax import lax
from jax.experimental import pallas as pl
from jax.experimental.pallas import tpu as pltpu
from jax.sharding import PartitionSpec as P

HEADS = 8
KVH = 2
GRID_W = 64
EPSILON = 1e-06
THETA = 10000.0
LANES = 128
MESH = pl.DeviceIdType.MESH
F32 = jnp.float32
BF16 = jnp.bfloat16


def rotary_tables(seq_total, head_dim):
    quarter = head_dim // 4
    inverse = np.float32(THETA) ** (
        -(np.float32(2.0) * np.arange(quarter, dtype=np.float32)) / np.float32(head_dim // 2)
    )
    inverse = inverse.astype(np.float32)
    rows = (np.arange(seq_total // GRID_W) - seq_total // GRID_W // 2).astype(np.float32)
    cols = (np.arange(GRID_W) - GRID_W // 2).astype(np.float32)
    sign = np.where((np.arange(head_dim) // quarter) % 2 == 0, -1.0, 1.0).astype(np.float32)

    def tables(positions):
        angle = np.tile((positions[:, None] * inverse[None, :]).astype(np.float32), (1, 4))
        angle = angle.astype(np.float64)
        return np.stack([np.cos(angle), np.sin(angle) * sign]).astype(np.float32)

    return tables(rows), tables(cols)


def ring_kernel(
    n_sp,
    n_tp,
    row_tab,
    col_tab,
    q_ref,
    k_ref,
    v_ref,
    qg_ref,
    kg_ref,
    res_ref,
    ow_ref,
    mg_ref,
    fg_ref,
    g_ref,
    u_ref,
    d_ref,
    cg_ref,
    cv_ref,
    out_ref,
    kv,
    q_rot,
    top,
    den,
    acc,
    att_own,
    att_all,
    ow_all,
    mix,
    stream,
    normed,
    wbuf,
    ups,
    hidden,
    part,
    red,
    kv_s,
    kv_r,
    sib_s,
    sib_r,
    w_s,
    w_r,
    y_s,
    y_r,
    ow_s,
    ow_r,
    nm_s,
    nm_r,
    a2a_s,
    a2a_r,
    halo_s,
    halo_r,
    red_s,
    red_r,
):
    half = n_sp // 2
    n_x = n_tp // 2
    tok = q_ref.shape[0]
    own = res_ref.shape[0]
    model = res_ref.shape[1]
    units = g_ref.shape[0]
    common = units // 3 // 16 * 16
    private = (units - common) // 2
    piece_tok = tok // 2
    sources = (g_ref, u_ref, d_ref)

    g = lax.axis_index("grp")
    s = lax.axis_index("sp")
    t = lax.axis_index("tp")
    x, c = t // 2, t % 2
    z_right, z_left = (s + 1) % n_sp, (s + n_sp - 1) % n_sp
    partner = g + 1 - 2 * (g % 2)
    sibling = t + 1 - 2 * c
    x_right = 2 * ((x + 1) % n_x) + c
    x_left = 2 * ((x + n_x - 1) % n_x) + c
    kv_head = t // (HEADS // KVH)

    barrier = pltpu.get_barrier_semaphore()
    peers = [{"sp": z_right}, {"sp": z_left}, {"grp": partner}]
    peers += [{"tp": (t + i) % n_tp} for i in range(1, n_tp)]
    for peer in peers:
        pl.semaphore_signal(barrier, inc=1, device_id=peer, device_id_type=MESH)

    def remote(src, dst, send, recv, device):
        return pltpu.make_async_remote_copy(
            src_ref=src,
            dst_ref=dst,
            send_sem=send,
            recv_sem=recv,
            device_id=device,
            device_id_type=MESH,
        )

    def block_of(direction, step):
        return (s + n_sp - step) % n_sp if direction == 0 else (s + step) % n_sp

    def z_device(direction):
        return {"sp": z_right if direction == 0 else z_left}

    def kv_at(which, block, piece):
        start = pl.multiple_of(block * tok + piece * piece_tok, piece_tok)
        return kv.at[which, pl.ds(start, piece_tok), :]

    def kv_copy(direction, step, piece, block):
        ref = kv_at(c, block, piece)
        i = (direction * half + step) * 2 + piece
        return remote(ref, ref, kv_s.at[i], kv_r.at[i], z_device(direction))

    def sib_copy(which, direction, step, piece, block):
        ref = kv_at(which, block, piece)
        i = (direction * half + step) * 2 + piece
        return remote(ref, ref, sib_s.at[i], sib_r.at[i], {"tp": sibling})

    def w_rows(piece):
        if piece == 0:
            return pl.ds(pl.multiple_of((g % 2) * (private + common), 16), private)
        return pl.ds(private, common)

    def w_at(a, block, rows):
        return wbuf.at[a, rows, pl.ds(pl.multiple_of(block * LANES, LANES), LANES)]

    def w_copy(a, direction, step, piece, block, first=False):
        rows = w_rows(piece)
        dst = w_at(a, block, rows)
        src = sources[a].at[rows, :] if first else dst
        i = ((a * 2 + direction) * half + step) * 2 + piece
        return remote(src, dst, w_s.at[i], w_r.at[i], z_device(direction))

    def y_copy(a, direction, step, block, mine):
        side = g % 2 if mine else 1 - g % 2
        rows = pl.ds(pl.multiple_of(side * (private + common), 16), private)
        ref = w_at(a, block, rows)
        i = (a * 2 + direction) * half + step
        return remote(ref, ref, y_s.at[i], y_r.at[i], {"grp": partner})

    def w_start(arrays):
        for piece in range(2):
            for a in arrays:
                for direction in range(2):
                    w_copy(a, direction, 0, piece, s, first=True).start()

    def when(condition):
        if isinstance(condition, bool):
            return (lambda f: f()) if condition else (lambda f: None)
        return pl.when(condition)

    def w_serve(arrays, k):
        for piece in range(2):
            for a in arrays:
                for direction in range(2):
                    last = direction == piece
                    block = block_of(direction, k)

                    @when(k <= half if last else k < half)
                    def _():
                        w_copy(a, direction, k - 1, piece, block).wait_recv()

                        @when(k <= half - 1 if last else k <= half - 2)
                        def _():
                            w_copy(a, direction, k, piece, block).start()

                        if piece == 0:
                            y_copy(a, direction, k - 1, block, True).start()

    def x_gather(buf, rows, first, send, recv):
        hold = rows // 2

        def at(block, lo, size):
            return buf.at[pl.ds(pl.multiple_of(block * rows + lo, 16), size), :]

        def ring(direction, step, chip, lo, size, src=None):
            dst = at(2 * chip + c, lo, size)
            i = direction * 2 + step
            device = {"tp": x_right if direction == 0 else x_left}
            return remote(dst if src is None else src, dst, send.at[i], recv.at[i], device)

        def share(i, chip, core, lo, size, src=None):
            dst = at(2 * chip + core, lo, size)
            return remote(
                dst if src is None else src, dst, send.at[4 + i], recv.at[4 + i], {"tp": sibling}
            )

        chips = ((x + n_x - 1) % n_x, (x + 1) % n_x)
        far = (x + 2) % n_x

        def start():
            for direction in range(2):
                ring(direction, 0, x, 0, rows, first).start()
            share(4, x, c, 0, rows, first).start()

        def middle():
            for direction in range(2):
                chip = chips[direction]
                ring(direction, 0, chip, 0, rows).wait_recv()
                ring(direction, 1, chip, direction * hold, hold).start()
                share(direction, chip, c, 0, rows).start()

        def end():
            for direction in range(2):
                ring(direction, 1, far, direction * hold, hold).wait_recv()
                share(2 + direction, far, c, direction * hold, hold).start()

        def arrived():
            other = 1 - c
            share(4, x, other, 0, rows).wait_recv()
            for direction in range(2):
                share(direction, chips[direction], other, 0, rows).wait_recv()
                share(2 + direction, far, other, direction * hold, hold).wait_recv()

        def sent():
            for direction in range(2):
                ring(direction, 0, x, 0, rows, first).wait_send()
                ring(direction, 1, chips[direction], direction * hold, hold).wait_send()
                share(direction, chips[direction], c, 0, rows).wait_send()
                share(2 + direction, far, c, direction * hold, hold).wait_send()
            share(4, x, c, 0, rows, first).wait_send()

        return start, middle, end, arrived, sent

    ow_start, ow_middle, ow_end, ow_arrived, ow_sent = x_gather(
        ow_all, ow_ref.shape[0], ow_ref, ow_s, ow_r
    )
    nm_start, nm_middle, nm_end, nm_arrived, nm_sent = x_gather(normed, own, None, nm_s, nm_r)

    grid_rows = tok // GRID_W
    lane = lax.broadcasted_iota(jnp.int32, (GRID_W, LANES), 1)
    quarter = LANES // 4

    def prepare(raw, gain, grid_row, factor):
        floats = raw.astype(F32)
        mean = jnp.sum(floats * floats, axis=-1, keepdims=True) * (1.0 / LANES)
        n = floats * lax.rsqrt(mean + EPSILON) * gain
        at = s * grid_rows + grid_row
        cos = jnp.where(lane < LANES // 2, row_tab[0, pl.ds(at, 1), :], col_tab[0])
        sin = jnp.where(lane < LANES // 2, row_tab[1, pl.ds(at, 1), :], col_tab[1])
        turned = jnp.where(
            (lane // quarter) % 2 == 0,
            pltpu.roll(n, LANES - quarter, 1),
            pltpu.roll(n, quarter, 1),
        )
        return ((n * cos + turned * sin) * factor).astype(BF16)

    head_cols = pl.ds(pl.multiple_of(kv_head * LANES, LANES), LANES)

    @pl.loop(0, grid_rows)
    def _(r):
        rows = pl.ds(pl.multiple_of(r * GRID_W, GRID_W), GRID_W)
        into = pl.ds(pl.multiple_of(s * tok + r * GRID_W, GRID_W), GRID_W)
        kv[0, into, :] = prepare(k_ref[rows, head_cols], kg_ref[...], r, 1.0)
        kv[1, into, :] = v_ref[rows, head_cols]

    pl.semaphore_wait(barrier, len(peers))
    for piece in range(2):
        for direction in range(2):
            kv_copy(direction, 0, piece, s).start()
    ow_start()

    @pl.loop(0, grid_rows)
    def _(r):
        rows = pl.ds(pl.multiple_of(r * GRID_W, GRID_W), GRID_W)
        q_rot[rows, :] = prepare(q_ref[rows, :], qg_ref[...], r, LANES ** (-0.5))

    top[...] = jnp.full_like(top, -1e30)
    den[...] = jnp.zeros_like(den)
    acc[...] = jnp.zeros_like(acc)
    for a in range(3):
        wbuf[a, :, pl.ds(pl.multiple_of(s * LANES, LANES), LANES)] = sources[a][...]
    ow_rows = ow_ref.shape[0]
    ow_all[pl.ds(pl.multiple_of(t * ow_rows, 16), ow_rows), :] = ow_ref[...]

    chunk = min(256, tok)

    def attend(block):
        keys = pl.ds(pl.multiple_of(block * tok, tok), tok)

        @pl.loop(0, tok // chunk)
        def _(i):
            rows = pl.ds(pl.multiple_of(i * chunk, chunk), chunk)
            scores = lax.dot_general(
                q_rot[rows, :],
                kv[0, keys, :],
                (((1,), (1,)), ((), ())),
                preferred_element_type=F32,
            )
            before = top[rows, :]
            newest = jnp.maximum(before, jnp.max(scores, axis=1, keepdims=True))
            wide = jnp.concatenate([newest] * (tok // LANES), axis=1)
            weights = jnp.exp(scores - wide)
            fade = jnp.exp(before - newest)
            den[rows, :] = den[rows, :] * fade + jnp.sum(weights, axis=1, keepdims=True)
            acc[rows, :] = acc[rows, :] * fade + jnp.dot(
                weights.astype(BF16), kv[1, keys, :], preferred_element_type=F32
            )
            top[rows, :] = newest

    @pl.loop(1, half + 2)
    def _(k):
        for piece in range(2):
            for direction in range(2):
                last = direction == piece
                block = block_of(direction, k)

                @pl.when(k <= half if last else k < half)
                def _():
                    kv_copy(direction, k - 1, piece, block).wait_recv()

                    @pl.when(k <= half - 1 if last else k <= half - 2)
                    def _():
                        kv_copy(direction, k, piece, block).start()

                    sib_copy(c, direction, k - 1, piece, block).start()

        @pl.when(k == half - 1)
        def _():
            w_start((0, 1))

        @pl.when(k == half // 2)
        def _():
            ow_middle()

        @pl.when(k == half - 1)
        def _():
            ow_end()

        for piece in range(2):
            for direction in range(2):
                last = direction == piece
                block = block_of(direction, k - 1)

                @pl.when((k >= 2) & (k <= half + 1 if last else k <= half))
                def _():
                    sib_copy(1 - c, direction, k - 2, piece, block).wait_recv()

        @pl.loop(0, jnp.where((k == 1) | (k == half + 1), 1, 2))
        def _(i):
            attend((s + n_sp + (k - 1) * (2 * i - 1)) % n_sp)

    w_serve((0, 1), 1)
    att_own[...] = (acc[...] / den[...]).astype(BF16)

    def att_copy(i, to, source):
        cols = pl.ds(pl.multiple_of(source * LANES, LANES), LANES)
        rows = pl.ds(pl.multiple_of(to * own, 16), own)
        return remote(
            att_own.at[rows, :],
            att_all.at[:, cols],
            a2a_s.at[i - 1],
            a2a_r.at[i - 1],
            {"tp": to},
        )

    for i in range(1, n_tp):
        att_copy(i, (t + i) % n_tp, t).start()
    att_all[:, pl.ds(pl.multiple_of(t * LANES, LANES), LANES)] = att_own[
        pl.ds(pl.multiple_of(t * own, 16), own), :
    ]
    ow_arrived()
    w_serve((0, 1), 2)
    for i in range(1, n_tp):
        att_copy(i, t, (t + n_tp - i) % n_tp).wait_recv()

    width = min(512, model)

    @pl.loop(0, model // width)
    def _(j):
        cols = pl.ds(pl.multiple_of(j * width, width), width)
        total = jnp.zeros((own, width), F32)
        for head in range(n_tp):
            span = slice(head * LANES, (head + 1) * LANES)
            total += (
                jnp.dot(att_all[:, span], ow_all[span, cols], preferred_element_type=F32)
                .astype(BF16)
                .astype(F32)
            )
        mix[:, cols] = total

    @pl.loop(0, own // 16)
    def _(r):
        rows = pl.ds(pl.multiple_of(r * 16, 16), 16)
        m = mix[rows, :]
        scale = lax.rsqrt(jnp.mean(m * m, axis=-1, keepdims=True) + EPSILON)
        added = (res_ref[rows, :].astype(F32) + m * scale * mg_ref[...]).astype(BF16)
        stream[rows, :] = added
        f = added.astype(F32)
        scale = lax.rsqrt(jnp.mean(f * f, axis=-1, keepdims=True) + EPSILON)
        normed[pl.ds(pl.multiple_of(t * own + r * 16, 16), 16), :] = (
            f * scale * fg_ref[...]
        ).astype(BF16)

    served = min(3, half)
    if served == 3:
        w_serve((0, 1), 3)
    nm_start()
    for k in range(served + 1, half + 1):
        w_serve((0, 1), k)
        if k == half - 1:
            w_start((2,))
        if k == served + 1:
            nm_middle()
        if k == served + 3:
            nm_end()
    if half < served + 1:
        w_start((2,))
        nm_middle()
        nm_end()
    elif half < served + 3:
        nm_end()
    nm_arrived()

    def y_arrived(a, direction, step):
        y_copy(a, direction, step, block_of(direction, step + 1), False).wait_recv()

    for a in range(2):
        for step in range(half):
            for direction in range(2 if step < half - 1 else 1):
                y_arrived(a, direction, step)

    m_rows = min(256, tok)
    m_count = tok // m_rows

    @pl.loop(0, m_count)
    def _(i):
        rows = pl.ds(pl.multiple_of(i * m_rows, m_rows), m_rows)
        for a in range(2):
            made = lax.dot_general(
                normed[rows, :],
                wbuf[a],
                (((1,), (1,)), ((), ())),
                preferred_element_type=F32,
            )
            ups[a, pl.ds(pl.multiple_of(8 + i * m_rows, 8), m_rows), :] = made.astype(BF16).astype(
                F32
            )

        @pl.when(i + 1 <= half)
        def _():
            w_serve((2,), i + 1)

    done = min(m_count, half)

    def halo_copy(direction):
        if direction == 0:
            src, dst = ups.at[:, pl.ds(tok, 8), :], ups.at[:, pl.ds(0, 8), :]
        else:
            src, dst = ups.at[:, pl.ds(8, 8), :], ups.at[:, pl.ds(tok + 8, 8), :]
        return remote(src, dst, halo_s.at[direction], halo_r.at[direction], z_device(direction))

    for direction in range(2):
        halo_copy(direction).start()

    c_rows = min(32, tok)
    c_count = tok // c_rows
    every = max(c_count // 4, 1)

    @pl.loop(0, c_count)
    def _(i):
        at = (i + 1) % c_count

        @pl.when(i == c_count - 2)
        def _():
            for direction in range(2):
                halo_copy(direction).wait_recv()
            ups[:, pl.ds(0, 8), :] = jnp.where(s == 0, 0.0, ups[:, pl.ds(0, 8), :])
            ups[:, pl.ds(tok + 8, 8), :] = jnp.where(
                s == n_sp - 1, 0.0, ups[:, pl.ds(tok + 8, 8), :]
            )

        mixed = []
        for a, taps in ((0, cg_ref), (1, cv_ref)):
            near = ups[a, pl.ds(pl.multiple_of(at * c_rows, c_rows), c_rows + 16), :]
            mixed.append(
                taps[0:1, :] * near[7 : 7 + c_rows]
                + taps[1:2, :] * near[8 : 8 + c_rows]
                + taps[2:3, :] * near[9 : 9 + c_rows]
            )
        v = mixed[0]
        inner = (2.0 / np.pi) ** 0.5 * (v + 0.044715 * (v * v * v))
        gated = 0.5 * v * (1.0 + jnp.tanh(inner)) * mixed[1]
        hidden[pl.ds(pl.multiple_of(at * c_rows, c_rows), c_rows), :] = gated.astype(BF16)

        @pl.when((i % every == every - 1) & (done + 1 + i // every <= half))
        def _():
            w_serve((2,), done + 1 + i // every)

    done = min(half, done + c_count // every)

    def red_copy(i, to, source, block):
        rows = pl.ds(pl.multiple_of(to * own, 16), own)
        return remote(
            part.at[block, rows, :],
            red.at[source, block],
            red_s.at[i - 1],
            red_r.at[i - 1],
            {"tp": to},
        )

    def red_all(i, source):
        return remote(
            red.at[source], red.at[source], red_s.at[i - 1], red_r.at[i - 1], {"tp": source}
        )

    @pl.loop(1, half + 1)
    def _(j):
        @pl.when(j > done)
        def _():
            w_serve((2,), j)

        y_arrived(2, 0, j - 1)

        @pl.when(j < half)
        def _():
            y_arrived(2, 1, j - 1)

        first, second = (s + n_sp - j) % n_sp, (s + j % half) % n_sp

        def cols(block):
            return pl.ds(pl.multiple_of(block * LANES, LANES), LANES)

        @pl.loop(0, m_count)
        def _(i):
            rows = pl.ds(pl.multiple_of(i * m_rows, m_rows), m_rows)
            both = jnp.concatenate([wbuf[2, :, cols(first)], wbuf[2, :, cols(second)]], axis=1)
            made = jnp.dot(hidden[rows, :], both, preferred_element_type=F32).astype(BF16)
            part[first, rows, :] = made[:, :LANES]
            part[second, rows, :] = made[:, LANES:]

        for i in range(1, n_tp):
            to = (t + i) % n_tp
            red_copy(i, to, t, first).start()
            red_copy(i, to, t, second).start()

    for i in range(1, n_tp):
        red_all(i, (t + n_tp - i) % n_tp).wait_recv()

    own_rows = pl.ds(pl.multiple_of(t * own, 16), own)
    for b in range(n_sp):
        span = slice(b * LANES, (b + 1) * LANES)
        total = part[b, own_rows, :].astype(F32)
        for i in range(1, n_tp):
            total += red[(t + n_tp - i) % n_tp, b].astype(F32)
        out_ref[:, span] = (stream[:, span].astype(F32) + total).astype(BF16)

    ow_sent()
    nm_sent()
    for i in range(1, n_tp):
        att_copy(i, (t + i) % n_tp, t).wait_send()
        red_all(i, (t + i) % n_tp).wait_send()
    for direction in range(2):
        halo_copy(direction).wait_send()
        for step in range(half):
            for piece in range(2):
                if step == half - 1 and direction != piece:
                    continue
                block = block_of(direction, step)
                kv_copy(direction, step, piece, block).wait_send()
                sib_copy(c, direction, step, piece, block_of(direction, step + 1)).wait_send()
                for a in range(3):
                    w_copy(a, direction, step, piece, block, first=step == 0).wait_send()
                    if piece == 0:
                        y_copy(
                            a, direction, step, block_of(direction, step + 1), True
                        ).wait_send()


def body(
    queries,
    keys,
    values,
    query_gain,
    key_gain,
    residual,
    out_weight,
    mix_gain,
    ffn_gain,
    gate_in,
    value_in,
    conv_gate,
    conv_value,
    down_t,
):
    n_sp, n_tp = lax.axis_size("sp"), lax.axis_size("tp")
    half = n_sp // 2
    tok = queries.shape[0]
    own, model = residual.shape
    units = gate_in.shape[1]
    row_tab, col_tab = rotary_tables(tok * n_sp, query_gain.shape[0])
    vmem = pl.BlockSpec(memory_space=pltpu.VMEM)
    dma = pltpu.SemaphoreType.DMA
    operands = (
        jnp.asarray(row_tab),
        jnp.asarray(col_tab),
        queries,
        keys,
        values,
        query_gain[None, :],
        key_gain[None, :],
        residual,
        out_weight,
        mix_gain[None, :],
        ffn_gain[None, :],
        gate_in.T,
        value_in.T,
        down_t.T,
        conv_gate,
        conv_value,
    )
    return pl.pallas_call(
        functools.partial(ring_kernel, n_sp, n_tp),
        out_shape=jax.ShapeDtypeStruct((own, model), BF16),
        in_specs=[vmem] * len(operands),
        out_specs=vmem,
        scratch_shapes=[
            pltpu.VMEM((2, tok * n_sp, LANES), BF16),
            pltpu.VMEM((tok, LANES), BF16),
            pltpu.VMEM((tok, LANES), F32),
            pltpu.VMEM((tok, LANES), F32),
            pltpu.VMEM((tok, LANES), F32),
            pltpu.VMEM((tok, LANES), BF16),
            pltpu.VMEM((own, n_tp * LANES), BF16),
            pltpu.VMEM((n_tp * out_weight.shape[0], model), BF16),
            pltpu.VMEM((own, model), F32),
            pltpu.VMEM((own, model), BF16),
            pltpu.VMEM((tok, model), BF16),
            pltpu.VMEM((3, units, model), BF16),
            pltpu.VMEM((2, tok + 16, units), F32),
            pltpu.VMEM((tok, units), BF16),
            pltpu.VMEM((n_sp, tok, LANES), BF16),
            pltpu.VMEM((n_tp, n_sp, own, LANES), BF16),
            dma((4 * half,)),
            dma((4 * half,)),
            dma((4 * half,)),
            dma((4 * half,)),
            dma((12 * half,)),
            dma((12 * half,)),
            dma((6 * half,)),
            dma((6 * half,)),
            dma((9,)),
            dma((9,)),
            dma((9,)),
            dma((9,)),
            dma((n_tp - 1,)),
            dma((n_tp - 1,)),
            dma((2,)),
            dma((2,)),
            dma((n_tp - 1,)),
            dma((n_tp - 1,)),
        ],
        compiler_params=pltpu.CompilerParams(
            collective_id=0,
            has_side_effects=True,
            vmem_limit_bytes=62 * 1024 * 1024,
        ),
        name="layer",
    )(*operands)


def solution(mesh):
    return jax.shard_map(
        body,
        mesh=mesh,
        in_specs=(
            P(("grp", "sp"), "tp"),
            P(("grp", "sp"), None),
            P(("grp", "sp"), None),
            P(),
            P(),
            P(("grp", "sp", "tp"), None),
            P("tp", None),
            P(),
            P(),
            P("sp", "tp"),
            P("sp", "tp"),
            P(None, "tp"),
            P(None, "tp"),
            P("sp", "tp"),
        ),
        out_specs=P(("grp", "sp", "tp"), None),
        check_vma=False,
    )
```

time: 346 us -> 179 us (0.52)
  Pallas kernels: 0 us -> 177 us
  waiting for transfers between devices: 161 us -> 0 us
  blocking collectives: 87.7 us -> 0 us
  matrix products: 48.5 us -> 0 us
  other arithmetic: 28.9 us -> 0 us
  between operations: 13.4 us -> 0.01 us
  starting transfers between devices: 4.63 us -> 0 us
    pallas_call x0 -> x1, Pallas kernels: none -> 177 us  [body(): pl.pallas_call(functools.partial(ring_kernel, n_sp, n_tp), out_shape=jax....]
    all_gather x3 -> x0, waiting for transfers between devices: 158 us -> none  [the longest x2 116 us: sent_together(): lax.all_gather(both, axis, axis=dim, tiled=True)]
    all_to_all x2 -> x0, blocking collectives: 87.7 us -> none  [summed_on_arrival(): lax.all_to_all(tiles, axis, split_axis=0, concat_axis=0, tiled=True)]
    dot_general x4 -> x0, matrix products: 48.5 us -> none  [the longest x1 18.7 us: body(): jnp.dot(block_rows, out_weight, preferred_element_type=jnp.float32)]
    reduce_sum x7 -> x0, other arithmetic: 18.3 us -> none  [the longest x1 15.4 us: body(): denom = jnp.sum(weights, axis=1, keepdims=True)]
    ppermute x2 -> x0, starting transfers between devices: 4.5 us -> none  [the longest x1 3.19 us: with_halo(): lax.ppermute(lax.slice_in_dim(block, block.shape[dim] - width, None, axis...]
    convert_element_type x5 -> x0, other arithmetic: 4.18 us -> none  [the longest x1 1.97 us: prepare_heads(): return (turned * factor).astype(jnp.bfloat16)]
  transfers between devices with their start and end apart: 5 -> 0, of which waited for: 4 -> 0; matrix products, arithmetic and copies ran while one was open for 16% -> 0% of each run, Pallas kernels for 0% -> 0%
where the time goes in v1:
time: 179 us
  Pallas kernels  177 us (99%)
    pallas_call x1, Pallas kernels, body(): pl.pallas_call(functools.partial(ring_kernel, n_sp, n_tp), out_shape=jax....  177 us

profile of v1, /device:TPU:33, one launch (start us, length us, event | category | flops | bytes accessed | tf_op | source)
XLA Modules:
  0.0 178.6 jit_solution(1478058678923758571)
XLA Ops:
  0.0 176.8 %layer.1 = bf16[96,2048]{1,0:T(8,128)(2,1)} custom-call(f32[2,192,128]{2,1,0:T(8,128)} %constant.4.clone.row_tab, f32[2,64,128]{2,1,0:T(8,128)} %constant.5.clone.col_tab, bf16[768,128]{1,0:T(8,128)(2,1)} %q_ref.1, bf16[768,256]{1,0:T(8,128)(2,1)} %k_ref.1, bf16[768,256]{1,0:T(8,128)(2,1)} %v_ref.1, f32[1,128]{1,0:T(1,128)} %bitcast.12, f32[1,128]{1,0:T(1,128)} %bitcast.13, ...), custom_call_target="tpu_custom_call" | custom-call | tf_op jit(solution)/shard_map/layer/pallas_call | solution.py:646
  176.8 1.8 copy.18

commit v2 on v1

--- a/solution.py
+++ b/solution.py
@@ -72,11 +72,18 @@
     ups,
     hidden,
     part,
-    red,
+    pair_in,
+    pair_sum,
+    far_in,
+    near_in,
     kv_s,
     kv_r,
     sib_s,
     sib_r,
+    xp_s,
+    xp_r,
+    rel_s,
+    rel_r,
     w_s,
     w_r,
     y_s,
@@ -89,8 +96,12 @@
     a2a_r,
     halo_s,
     halo_r,
-    red_s,
-    red_r,
+    pair_s,
+    pair_r,
+    far_s,
+    far_r,
+    near_s,
+    near_r,
 ):
     half = n_sp // 2
     n_x = n_tp // 2
@@ -100,7 +111,8 @@
     units = g_ref.shape[0]
     common = units // 3 // 16 * 16
     private = (units - common) // 2
-    piece_tok = tok // 2
+    kv_common = tok // 3 // 32 * 32
+    kv_private = (tok - kv_common) // 2
     sources = (g_ref, u_ref, d_ref)
 
     g = lax.axis_index("grp")
@@ -113,6 +125,8 @@
     x_right = 2 * ((x + 1) % n_x) + c
     x_left = 2 * ((x + n_x - 1) % n_x) + c
     kv_head = t // (HEADS // KVH)
+    x_pair = x + 1 - 2 * (x % 2)
+    x_cross = (x + n_x - 1 + 2 * (x % 2)) % n_x
 
     barrier = pltpu.get_barrier_semaphore()
     peers = [{"sp": z_right}, {"sp": z_left}, {"grp": partner}]
@@ -136,19 +150,32 @@
     def z_device(direction):
         return {"sp": z_right if direction == 0 else z_left}
 
-    def kv_at(which, block, piece):
-        start = pl.multiple_of(block * tok + piece * piece_tok, piece_tok)
-        return kv.at[which, pl.ds(start, piece_tok), :]
+    def kv_at(which, block, piece, side):
+        if piece == 0:
+            start, size = side * (kv_private + kv_common), kv_private
+        else:
+            start, size = kv_private, kv_common
+        return kv.at[which, pl.ds(pl.multiple_of(block * tok + start, 16), size), :]
 
     def kv_copy(direction, step, piece, block):
-        ref = kv_at(c, block, piece)
+        ref = kv_at(c, block, piece, x % 2)
         i = (direction * half + step) * 2 + piece
         return remote(ref, ref, kv_s.at[i], kv_r.at[i], z_device(direction))
 
     def sib_copy(which, direction, step, piece, block):
-        ref = kv_at(which, block, piece)
+        ref = kv_at(which, block, piece, x % 2)
         i = (direction * half + step) * 2 + piece
         return remote(ref, ref, sib_s.at[i], sib_r.at[i], {"tp": sibling})
+
+    def xp_copy(direction, step, block, mine):
+        ref = kv_at(c, block, 0, x % 2 if mine else 1 - x % 2)
+        i = direction * half + step
+        return remote(ref, ref, xp_s.at[i], xp_r.at[i], {"tp": 2 * x_pair + c})
+
+    def rel_copy(which, direction, step, block):
+        ref = kv_at(which, block, 0, 1 - x % 2)
+        i = direction * half + step
+        return remote(ref, ref, rel_s.at[i], rel_r.at[i], {"tp": sibling})
 
     def w_rows(piece):
         if piece == 0:
@@ -183,14 +210,14 @@
             return (lambda f: f()) if condition else (lambda f: None)
         return pl.when(condition)
 
-    def w_serve(arrays, k):
-        for piece in range(2):
+    def w_serve(arrays, k, pieces=(0, 1)):
+        for piece in pieces:
             for a in arrays:
                 for direction in range(2):
                     last = direction == piece
                     block = block_of(direction, k)
 
-                    @when(k <= half if last else k < half)
+                    @when((k >= 1) & (k <= half if last else k < half))
                     def _():
                         w_copy(a, direction, k - 1, piece, block).wait_recv()
 
@@ -256,9 +283,52 @@
 
         return start, middle, end, arrived, sent
 
-    ow_start, ow_middle, ow_end, ow_arrived, ow_sent = x_gather(
-        ow_all, ow_ref.shape[0], ow_ref, ow_s, ow_r
-    )
+    ow_rows = ow_ref.shape[0]
+    ow_parts = 4
+    ow_far = x_cross + 1 - 2 * (x_cross % 2)
+
+    def ow_copy(i, chip, core, lo, size, device, first=False):
+        dst = ow_all.at[pl.ds(pl.multiple_of((2 * chip + core) * ow_rows + lo, 16), size), :]
+        src = ow_ref.at[pl.ds(lo, size), :] if first else dst
+        return remote(src, dst, ow_s.at[i], ow_r.at[i], {"tp": device})
+
+    size = ow_rows // ow_parts
+
+    def ow_pair(q, chip, first=False):
+        return ow_copy(q, chip, c, q * size, size, 2 * x_pair + c, first)
+
+    def ow_over(chip, first=False):
+        return ow_copy(4, chip, c, 0, ow_rows, 2 * x_cross + c, first)
+
+    def ow_on(q, chip):
+        return ow_copy(5 + q, chip, c, q * size, size, 2 * x_cross + c)
+
+    def ow_own(core, first=False):
+        return ow_copy(9, x, core, 0, ow_rows, sibling, first)
+
+    def ow_share(i, chip, core, lo, size):
+        return ow_copy(10 + i, chip, core, lo, size, sibling)
+
+    def ow_shares(core, i):
+        if i == 4:
+            return ow_share(4, x_cross, core, 0, ow_rows)
+        if i < 4:
+            return ow_share(i, x_pair, core, i * size, size)
+        return ow_share(i, ow_far, core, (i - 5) * size, size)
+
+    def ow_take(q):
+        ow_pair(q, x_pair).wait_recv()
+        ow_on(q, x_pair).start()
+        ow_shares(c, q).start()
+
+    def ow_across():
+        ow_over(x_cross).wait_recv()
+        ow_shares(c, 4).start()
+
+    def ow_take_far(q):
+        ow_on(q, ow_far).wait_recv()
+        ow_shares(c, 5 + q).start()
+
     nm_start, nm_middle, nm_end, nm_arrived, nm_sent = x_gather(normed, own, None, nm_s, nm_r)
 
     grid_rows = tok // GRID_W
@@ -292,7 +362,9 @@
     for piece in range(2):
         for direction in range(2):
             kv_copy(direction, 0, piece, s).start()
-    ow_start()
+    ow_over(x, first=True).start()
+    ow_own(c, first=True).start()
+    w_start((0,))
 
     @pl.loop(0, grid_rows)
     def _(r):
@@ -304,7 +376,6 @@
     acc[...] = jnp.zeros_like(acc)
     for a in range(3):
         wbuf[a, :, pl.ds(pl.multiple_of(s * LANES, LANES), LANES)] = sources[a][...]
-    ow_rows = ow_ref.shape[0]
     ow_all[pl.ds(pl.multiple_of(t * ow_rows, 16), ow_rows), :] = ow_ref[...]
 
     chunk = min(256, tok)
@@ -312,7 +383,7 @@
     def attend(block):
         keys = pl.ds(pl.multiple_of(block * tok, tok), tok)
 
-        @pl.loop(0, tok // chunk)
+        @pl.loop(0, tok // chunk, unroll=True)
         def _(i):
             rows = pl.ds(pl.multiple_of(i * chunk, chunk), chunk)
             scores = lax.dot_general(
@@ -332,9 +403,14 @@
             )
             top[rows, :] = newest
 
-    @pl.loop(1, half + 2)
+    @pl.loop(1, half + 3)
     def _(k):
-        for piece in range(2):
+        def at_step(step, act):
+            @pl.when(k == min(step, half + 2))
+            def _():
+                act()
+
+        def kv_serve(piece):
             for direction in range(2):
                 last = direction == piece
                 block = block_of(direction, k)
@@ -347,34 +423,61 @@
                     def _():
                         kv_copy(direction, k, piece, block).start()
 
+                    if piece == 0:
+                        xp_copy(direction, k - 1, block, True).start()
                     sib_copy(c, direction, k - 1, piece, block).start()
 
-        @pl.when(k == half - 1)
+        kv_serve(0)
+        for q in range(ow_parts):
+            at_step(1 + q, lambda: ow_pair(q, x, first=True).start())
+        w_serve((0,), k - 1, (0,))
+        for direction in range(2):
+            block = block_of(direction, k - 1)
+
+            @pl.when((k >= 2) & (k <= half + 1 if direction == 0 else k <= half))
+            def _():
+                xp_copy(direction, k - 2, block, False).wait_recv()
+                rel_copy(c, direction, k - 2, block).start()
+
+        for direction in range(2):
+            block = block_of(direction, k - 2)
+            for piece in range(2):
+                last = direction == piece
+
+                @pl.when((k >= 3) & (k <= half + 2 if last else k <= half + 1))
+                def _():
+                    sib_copy(1 - c, direction, k - 3, piece, block).wait_recv()
+
+            @pl.when((k >= 3) & (k <= half + 2 if direction == 0 else k <= half + 1))
+            def _():
+                rel_copy(1 - c, direction, k - 3, block).wait_recv()
+
+        @pl.when(k != 2)
         def _():
-            w_start((0, 1))
-
-        @pl.when(k == half // 2)
+            attend((s + n_sp - jnp.where(k == 1, 0, k - 2)) % n_sp)
+
+        kv_serve(1)
+        w_serve((0,), k - 1, (1,))
+        for q in range(ow_parts):
+            at_step(3 + q, lambda: ow_take(q))
+        at_step(5, ow_across)
+        for q in range(ow_parts):
+            at_step(7 + q, lambda: ow_take_far(q))
+        at_step(half, lambda: w_start((1,)))
+
+        @pl.when((k >= 3) & (k <= half + 1))
         def _():
-            ow_middle()
-
-        @pl.when(k == half - 1)
-        def _():
-            ow_end()
-
+            attend((s + k - 2) % n_sp)
+
+        at_step(half + 2, lambda: w_serve((1,), 1))
+
+    def vd_serve(k):
         for piece in range(2):
-            for direction in range(2):
-                last = direction == piece
-                block = block_of(direction, k - 1)
-
-                @pl.when((k >= 2) & (k <= half + 1 if last else k <= half))
-                def _():
-                    sib_copy(1 - c, direction, k - 2, piece, block).wait_recv()
-
-        @pl.loop(0, jnp.where((k == 1) | (k == half + 1), 1, 2))
-        def _(i):
-            attend((s + n_sp + (k - 1) * (2 * i - 1)) % n_sp)
-
-    w_serve((0, 1), 1)
+            w_serve((1,), k, (piece,))
+            w_serve((2,), k - 2, (piece,))
+        if k == 2:
+            w_start((2,))
+
     att_own[...] = (acc[...] / den[...]).astype(BF16)
 
     def att_copy(i, to, source):
@@ -393,8 +496,10 @@
     att_all[:, pl.ds(pl.multiple_of(t * LANES, LANES), LANES)] = att_own[
         pl.ds(pl.multiple_of(t * own, 16), own), :
     ]
-    ow_arrived()
-    w_serve((0, 1), 2)
+    for i in range(2 * ow_parts + 1):
+        ow_shares(1 - c, i).wait_recv()
+    ow_own(1 - c).wait_recv()
+    vd_serve(2)
     for i in range(1, n_tp):
         att_copy(i, t, (t + n_tp - i) % n_tp).wait_recv()
 
@@ -426,30 +531,20 @@
             f * scale * fg_ref[...]
         ).astype(BF16)
 
-    served = min(3, half)
-    if served == 3:
-        w_serve((0, 1), 3)
+    vd_serve(3)
     nm_start()
-    for k in range(served + 1, half + 1):
-        w_serve((0, 1), k)
-        if k == half - 1:
-            w_start((2,))
-        if k == served + 1:
-            nm_middle()
-        if k == served + 3:
-            nm_end()
-    if half < served + 1:
-        w_start((2,))
-        nm_middle()
-        nm_end()
-    elif half < served + 3:
-        nm_end()
+    vd_serve(4)
+    vd_serve(5)
+    nm_middle()
+    vd_serve(6)
+    nm_end()
+    vd_serve(7)
     nm_arrived()
 
     def y_arrived(a, direction, step):
         y_copy(a, direction, step, block_of(direction, step + 1), False).wait_recv()
 
-    for a in range(2):
+    def y_all(a):
         for step in range(half):
             for direction in range(2 if step < half - 1 else 1):
                 y_arrived(a, direction, step)
@@ -457,25 +552,33 @@
     m_rows = min(256, tok)
     m_count = tok // m_rows
 
+    def up(a, i):
+        rows = pl.ds(pl.multiple_of(i * m_rows, m_rows), m_rows)
+        made = lax.dot_general(
+            normed[rows, :], wbuf[a], (((1,), (1,)), ((), ())), preferred_element_type=F32
+        )
+        ups[a, pl.ds(pl.multiple_of(8 + i * m_rows, 8), m_rows), :] = made.astype(BF16).astype(F32)
+
+    y_all(0)
+
     @pl.loop(0, m_count)
     def _(i):
-        rows = pl.ds(pl.multiple_of(i * m_rows, m_rows), m_rows)
-        for a in range(2):
-            made = lax.dot_general(
-                normed[rows, :],
-                wbuf[a],
-                (((1,), (1,)), ((), ())),
-                preferred_element_type=F32,
-            )
-            ups[a, pl.ds(pl.multiple_of(8 + i * m_rows, 8), m_rows), :] = made.astype(BF16).astype(
-                F32
-            )
-
-        @pl.when(i + 1 <= half)
+        up(0, i)
+
+    for k in range(8, half + 1):
+        vd_serve(k)
+    done = min(max(half, 7) - 2, half)
+    y_all(1)
+
+    @pl.loop(0, m_count)
+    def _(i):
+        up(1, i)
+
+        @pl.when(done + 1 + i <= half)
         def _():
-            w_serve((2,), i + 1)
-
-    done = min(m_count, half)
+            w_serve((2,), done + 1 + i)
+
+    done = min(done + m_count, half)
 
     def halo_copy(direction):
         if direction == 0:
@@ -487,7 +590,13 @@
     for direction in range(2):
         halo_copy(direction).start()
 
-    c_rows = min(32, tok)
+    c_rows = min(32, own)
+
+    def by_core(row):
+        to = row // own
+        start = ((to % 2) * n_x + to // 2) * own + row % own
+        return pl.ds(pl.multiple_of(start, c_rows), c_rows)
+
     c_count = tok // c_rows
     every = max(c_count // 4, 1)
 
@@ -515,7 +624,7 @@
         v = mixed[0]
         inner = (2.0 / np.pi) ** 0.5 * (v + 0.044715 * (v * v * v))
         gated = 0.5 * v * (1.0 + jnp.tanh(inner)) * mixed[1]
-        hidden[pl.ds(pl.multiple_of(at * c_rows, c_rows), c_rows), :] = gated.astype(BF16)
+        hidden[by_core(at * c_rows), :] = gated.astype(BF16)
 
         @pl.when((i % every == every - 1) & (done + 1 + i // every <= half))
         def _():
@@ -523,68 +632,142 @@
 
     done = min(half, done + c_count // every)
 
-    def red_copy(i, to, source, block):
-        rows = pl.ds(pl.multiple_of(to * own, 16), own)
+    per_core = n_x * own
+    cut = own // 2
+    chip_right, chip_left = (x + 1) % n_x, (x + n_x - 1) % n_x
+    chip_far = (x + 2) % n_x
+
+    def pair_copy(i, block, core):
+        rows = pl.ds(pl.multiple_of(core * per_core, 16), per_core)
         return remote(
             part.at[block, rows, :],
-            red.at[source, block],
-            red_s.at[i - 1],
-            red_r.at[i - 1],
-            {"tp": to},
+            pair_in.at[block],
+            pair_s.at[i],
+            pair_r.at[i],
+            {"tp": sibling},
         )
 
-    def red_all(i, source):
+    def far_copy(direction, block):
+        lo = cut if direction == 0 else 0
         return remote(
-            red.at[source], red.at[source], red_s.at[i - 1], red_r.at[i - 1], {"tp": source}
+            pair_sum.at[block, pl.ds(pl.multiple_of(chip_far * own + lo, 16), cut), :],
+            far_in.at[direction, block],
+            far_s.at[direction * n_sp + block],
+            far_r.at[direction * n_sp + block],
+            {"tp": x_right if direction == 0 else x_left},
         )
 
-    @pl.loop(1, half + 1)
+    def near_copy(direction, block):
+        chip = chip_right if direction == 0 else chip_left
+        return remote(
+            pair_sum.at[block, pl.ds(pl.multiple_of(chip * own, 16), own), :],
+            near_in.at[direction, block],
+            near_s.at[direction],
+            near_r.at[direction],
+            {"tp": x_right if direction == 0 else x_left},
+        )
+
+    def near_all(direction):
+        ref = near_in.at[direction]
+        return remote(
+            ref,
+            ref,
+            near_s.at[direction],
+            near_r.at[direction],
+            {"tp": x_right if direction == 0 else x_left},
+        )
+
+    def of_core(chip, size, lo=0):
+        return pl.ds(pl.multiple_of(c * per_core + chip * own + lo, 16), size)
+
+    def of_chip(chip, size, lo=0):
+        return pl.ds(pl.multiple_of(chip * own + lo, 16), size)
+
+    def blocks(j):
+        return (s + n_sp - j) % n_sp, (s + j % half) % n_sp
+
+    @pl.loop(1, half + 3)
     def _(j):
-        @pl.when(j > done)
+        @pl.when(j <= half)
         def _():
-            w_serve((2,), j)
-
-        y_arrived(2, 0, j - 1)
-
-        @pl.when(j < half)
+            @pl.when(j > done)
+            def _():
+                w_serve((2,), j)
+
+            y_arrived(2, 0, j - 1)
+
+            @pl.when(j < half)
+            def _():
+                y_arrived(2, 1, j - 1)
+
+            first, second = blocks(j)
+
+            def cols(block):
+                return pl.ds(pl.multiple_of(block * LANES, LANES), LANES)
+
+            @pl.loop(0, m_count)
+            def _(i):
+                rows = pl.ds(pl.multiple_of(i * m_rows, m_rows), m_rows)
+                both = jnp.concatenate([wbuf[2, :, cols(first)], wbuf[2, :, cols(second)]], axis=1)
+                made = jnp.dot(hidden[rows, :], both, preferred_element_type=F32).astype(BF16)
+                part[first, rows, :] = made[:, :LANES]
+                part[second, rows, :] = made[:, LANES:]
+
+            for i, block in enumerate((first, second)):
+                pair_copy(2 * (j - 1) + i, block, 1 - c).start()
+
+        @pl.when((j >= 2) & (j <= half + 1))
         def _():
-            y_arrived(2, 1, j - 1)
-
-        first, second = (s + n_sp - j) % n_sp, (s + j % half) % n_sp
-
-        def cols(block):
-            return pl.ds(pl.multiple_of(block * LANES, LANES), LANES)
-
-        @pl.loop(0, m_count)
-        def _(i):
-            rows = pl.ds(pl.multiple_of(i * m_rows, m_rows), m_rows)
-            both = jnp.concatenate([wbuf[2, :, cols(first)], wbuf[2, :, cols(second)]], axis=1)
-            made = jnp.dot(hidden[rows, :], both, preferred_element_type=F32).astype(BF16)
-            part[first, rows, :] = made[:, :LANES]
-            part[second, rows, :] = made[:, LANES:]
-
-        for i in range(1, n_tp):
-            to = (t + i) % n_tp
-            red_copy(i, to, t, first).start()
-            red_copy(i, to, t, second).start()
-
-    for i in range(1, n_tp):
-        red_all(i, (t + n_tp - i) % n_tp).wait_recv()
-
-    own_rows = pl.ds(pl.multiple_of(t * own, 16), own)
+            for i, block in enumerate(blocks(j - 1)):
+                pair_copy(2 * (j - 2) + i, block, c).wait_recv()
+                for chip in (chip_far, chip_right, chip_left):
+                    pair_sum[block, of_chip(chip, own), :] = (
+                        part[block, of_core(chip, own), :].astype(F32)
+                        + pair_in[block, of_chip(chip, own), :].astype(F32)
+                    ).astype(BF16)
+                for direction in range(2):
+                    far_copy(direction, block).start()
+
+        @pl.when(j >= 3)
+        def _():
+            for block in blocks(j - 2):
+                for direction in range(2):
+                    far_copy(direction, block).wait_recv()
+                    chip = chip_right if direction == 0 else chip_left
+                    lo = cut if direction == 0 else 0
+                    pair_sum[block, of_chip(chip, cut, lo), :] = (
+                        part[block, of_core(chip, cut, lo), :].astype(F32)
+                        + pair_in[block, of_chip(chip, cut, lo), :].astype(F32)
+                        + far_in[direction, block].astype(F32)
+                    ).astype(BF16)
+                    near_copy(direction, block).start()
+
+    for direction in range(2):
+        near_all(direction).wait_recv()
+
     for b in range(n_sp):
         span = slice(b * LANES, (b + 1) * LANES)
-        total = part[b, own_rows, :].astype(F32)
-        for i in range(1, n_tp):
-            total += red[(t + n_tp - i) % n_tp, b].astype(F32)
+        total = part[b, of_core(x, own), :].astype(F32) + pair_in[b, of_chip(x, own), :].astype(F32)
+        for direction in range(2):
+            total += near_in[direction, b].astype(F32)
         out_ref[:, span] = (stream[:, span].astype(F32) + total).astype(BF16)
 
-    ow_sent()
+    for q in range(ow_parts):
+        ow_pair(q, x, first=True).wait_send()
+        ow_on(q, x_pair).wait_send()
+    ow_over(x, first=True).wait_send()
+    for i in range(2 * ow_parts + 1):
+        ow_shares(c, i).wait_send()
+    ow_own(c, first=True).wait_send()
     nm_sent()
     for i in range(1, n_tp):
         att_copy(i, (t + i) % n_tp, t).wait_send()
-        red_all(i, (t + i) % n_tp).wait_send()
+    for b in range(n_sp):
+        pair_copy(b, b, 1 - c).wait_send()
+        for direction in range(2):
+            far_copy(direction, b).wait_send()
     for direction in range(2):
+        near_all(direction).wait_send()
         halo_copy(direction).wait_send()
         for step in range(half):
             for piece in range(2):
@@ -593,6 +776,10 @@
                 block = block_of(direction, step)
                 kv_copy(direction, step, piece, block).wait_send()
                 sib_copy(c, direction, step, piece, block_of(direction, step + 1)).wait_send()
+                if piece == 0:
+                    arriving = block_of(direction, step + 1)
+                    xp_copy(direction, step, arriving, True).wait_send()
+                    rel_copy(c, direction, step, arriving).wait_send()
                 for a in range(3):
                     w_copy(a, direction, step, piece, block, first=step == 0).wait_send()
                     if piece == 0:
@@ -664,25 +851,36 @@
             pltpu.VMEM((2, tok + 16, units), F32),
             pltpu.VMEM((tok, units), BF16),
             pltpu.VMEM((n_sp, tok, LANES), BF16),
-            pltpu.VMEM((n_tp, n_sp, own, LANES), BF16),
+            pltpu.VMEM((n_sp, tok // 2, LANES), BF16),
+            pltpu.VMEM((n_sp, tok // 2, LANES), BF16),
+            pltpu.VMEM((2, n_sp, own // 2, LANES), BF16),
+            pltpu.VMEM((2, n_sp, own, LANES), BF16),
             dma((4 * half,)),
             dma((4 * half,)),
             dma((4 * half,)),
             dma((4 * half,)),
+            dma((2 * half,)),
+            dma((2 * half,)),
+            dma((2 * half,)),
+            dma((2 * half,)),
             dma((12 * half,)),
             dma((12 * half,)),
             dma((6 * half,)),
             dma((6 * half,)),
-            dma((9,)),
-            dma((9,)),
+            dma((19,)),
+            dma((19,)),
             dma((9,)),
             dma((9,)),
             dma((n_tp - 1,)),
             dma((n_tp - 1,)),
             dma((2,)),
             dma((2,)),
-            dma((n_tp - 1,)),
-            dma((n_tp - 1,)),
+            dma((n_sp,)),
+            dma((n_sp,)),
+            dma((2 * n_sp,)),
+            dma((2 * n_sp,)),
+            dma((2,)),
+            dma((2,)),
         ],
         compiler_params=pltpu.CompilerParams(
             collective_id=0,

time: 179 us -> 158 us (0.88)
  Pallas kernels: 177 us -> 156 us
    pallas_call x1, Pallas kernels: 177 us -> 156 us  [body(): pl.pallas_call(functools.partial(ring_kernel, n_sp, n_tp), out_shape=jax....]
where the time goes in v2:
time: 158 us
  Pallas kernels  156 us (99%)
  local copies, waits for them, and re-layouts  1.77 us (1%)
    pallas_call x1, Pallas kernels, body(): pl.pallas_call(functools.partial(ring_kernel, n_sp, n_tp), out_shape=jax....  156 us

profile of v2, /device:TPU:33, one launch (start us, length us, event | category | flops | bytes accessed | tf_op | source)
XLA Modules:
  0.0 158.3 jit_solution(5441725798146376417)
XLA Ops:
  0.0 156.5 %layer.1 = bf16[96,2048]{1,0:T(8,128)(2,1)} custom-call(f32[2,192,128]{2,1,0:T(8,128)} %constant.4.clone.row_tab, f32[2,64,128]{2,1,0:T(8,128)} %constant.5.clone.col_tab, bf16[768,128]{1,0:T(8,128)(2,1)} %q_ref.1, bf16[768,256]{1,0:T(8,128)(2,1)} %k_ref.1, bf16[768,256]{1,0:T(8,128)(2,1)} %v_ref.1, f32[1,128]{1,0:T(1,128)} %bitcast.12, f32[1,128]{1,0:T(1,128)} %bitcast.13, ...), custom_call_target="tpu_custom_call" | custom-call | tf_op jit(solution)/shard_map/layer/pallas_call | solution.py:833
  156.5 1.8 %copy.18 = bf16[96,2048]{1,0:T(8,128)(2,1)} copy(bf16[96,2048]{1,0:T(8,128)(2,1)} %layer.1) | data formatting | bytes 786432

commit v3 on v2

--- a/solution.py
+++ b/solution.py
@@ -70,6 +70,8 @@
     normed,
     wbuf,
     ups,
+    partial_up,
+    gated,
     hidden,
     part,
     pair_in,
@@ -109,9 +111,9 @@
     own = res_ref.shape[0]
     model = res_ref.shape[1]
     units = g_ref.shape[0]
-    common = units // 3 // 16 * 16
+    common = units * 4 // 11 // 16 * 16
     private = (units - common) // 2
-    kv_common = tok // 3 // 32 * 32
+    kv_common = tok // 4 // 32 * 32
     kv_private = (tok - kv_common) // 2
     sources = (g_ref, u_ref, d_ref)
 
@@ -177,26 +179,31 @@
         i = direction * half + step
         return remote(ref, ref, rel_s.at[i], rel_r.at[i], {"tp": sibling})
 
-    def w_rows(piece):
-        if piece == 0:
-            return pl.ds(pl.multiple_of((g % 2) * (private + common), 16), private)
-        return pl.ds(private, common)
+    def w_rows(a, piece, side):
+        if a == 0:
+            start, size = side * (units // 2) + piece * (units // 4), units // 4
+        elif piece == 0:
+            start, size = side * (private + common), private
+        else:
+            start, size = private, common
+        return pl.ds(pl.multiple_of(start, 16), size)
+
+    def over_y(a, piece):
+        return a == 0 or piece == 0
 
     def w_at(a, block, rows):
         return wbuf.at[a, rows, pl.ds(pl.multiple_of(block * LANES, LANES), LANES)]
 
     def w_copy(a, direction, step, piece, block, first=False):
-        rows = w_rows(piece)
+        rows = w_rows(a, piece, g % 2)
         dst = w_at(a, block, rows)
         src = sources[a].at[rows, :] if first else dst
         i = ((a * 2 + direction) * half + step) * 2 + piece
         return remote(src, dst, w_s.at[i], w_r.at[i], z_device(direction))
 
-    def y_copy(a, direction, step, block, mine):
-        side = g % 2 if mine else 1 - g % 2
-        rows = pl.ds(pl.multiple_of(side * (private + common), 16), private)
-        ref = w_at(a, block, rows)
-        i = (a * 2 + direction) * half + step
+    def y_copy(a, direction, step, piece, block, mine):
+        ref = w_at(a, block, w_rows(a, piece, g % 2 if mine else 1 - g % 2))
+        i = ((a * 2 + direction) * half + step) * 2 + piece
         return remote(ref, ref, y_s.at[i], y_r.at[i], {"grp": partner})
 
     def w_start(arrays):
@@ -225,8 +232,8 @@
                         def _():
                             w_copy(a, direction, k, piece, block).start()
 
-                        if piece == 0:
-                            y_copy(a, direction, k - 1, block, True).start()
+                        if over_y(a, piece):
+                            y_copy(a, direction, k - 1, piece, block, True).start()
 
     def x_gather(buf, rows, first, send, recv):
         hold = rows // 2
@@ -284,7 +291,7 @@
         return start, middle, end, arrived, sent
 
     ow_rows = ow_ref.shape[0]
-    ow_parts = 4
+    ow_parts = ow_rows // 16
     ow_far = x_cross + 1 - 2 * (x_cross % 2)
 
     def ow_copy(i, chip, core, lo, size, device, first=False):
@@ -298,23 +305,23 @@
         return ow_copy(q, chip, c, q * size, size, 2 * x_pair + c, first)
 
     def ow_over(chip, first=False):
-        return ow_copy(4, chip, c, 0, ow_rows, 2 * x_cross + c, first)
+        return ow_copy(ow_parts, chip, c, 0, ow_rows, 2 * x_cross + c, first)
 
     def ow_on(q, chip):
-        return ow_copy(5 + q, chip, c, q * size, size, 2 * x_cross + c)
+        return ow_copy(ow_parts + 1 + q, chip, c, q * size, size, 2 * x_cross + c)
 
     def ow_own(core, first=False):
-        return ow_copy(9, x, core, 0, ow_rows, sibling, first)
+        return ow_copy(2 * ow_parts + 1, x, core, 0, ow_rows, sibling, first)
 
     def ow_share(i, chip, core, lo, size):
-        return ow_copy(10 + i, chip, core, lo, size, sibling)
+        return ow_copy(2 * ow_parts + 2 + i, chip, core, lo, size, sibling)
 
     def ow_shares(core, i):
-        if i == 4:
-            return ow_share(4, x_cross, core, 0, ow_rows)
-        if i < 4:
+        if i == ow_parts:
+            return ow_share(i, x_cross, core, 0, ow_rows)
+        if i < ow_parts:
             return ow_share(i, x_pair, core, i * size, size)
-        return ow_share(i, ow_far, core, (i - 5) * size, size)
+        return ow_share(i, ow_far, core, (i - ow_parts - 1) * size, size)
 
     def ow_take(q):
         ow_pair(q, x_pair).wait_recv()
@@ -323,11 +330,11 @@
 
     def ow_across():
         ow_over(x_cross).wait_recv()
-        ow_shares(c, 4).start()
+        ow_shares(c, ow_parts).start()
 
     def ow_take_far(q):
         ow_on(q, ow_far).wait_recv()
-        ow_shares(c, 5 + q).start()
+        ow_shares(c, ow_parts + 1 + q).start()
 
     nm_start, nm_middle, nm_end, nm_arrived, nm_sent = x_gather(normed, own, None, nm_s, nm_r)
 
@@ -403,6 +410,7 @@
             )
             top[rows, :] = newest
 
+    ow_in_loop = min(ow_parts, max(half - 4, 0))
     @pl.loop(1, half + 3)
     def _(k):
         def at_step(step, act):
@@ -461,8 +469,8 @@
         for q in range(ow_parts):
             at_step(3 + q, lambda: ow_take(q))
         at_step(5, ow_across)
-        for q in range(ow_parts):
-            at_step(7 + q, lambda: ow_take_far(q))
+        for q in range(ow_in_loop):
+            at_step(6 + q, lambda: ow_take_far(q))
         at_step(half, lambda: w_start((1,)))
 
         @pl.when((k >= 3) & (k <= half + 1))
@@ -496,10 +504,12 @@
     att_all[:, pl.ds(pl.multiple_of(t * LANES, LANES), LANES)] = att_own[
         pl.ds(pl.multiple_of(t * own, 16), own), :
     ]
+    vd_serve(2)
+    for q in range(ow_in_loop, ow_parts):
+        ow_take_far(q)
     for i in range(2 * ow_parts + 1):
         ow_shares(1 - c, i).wait_recv()
     ow_own(1 - c).wait_recv()
-    vd_serve(2)
     for i in range(1, n_tp):
         att_copy(i, t, (t + n_tp - i) % n_tp).wait_recv()
 
@@ -541,54 +551,54 @@
     vd_serve(7)
     nm_arrived()
 
-    def y_arrived(a, direction, step):
-        y_copy(a, direction, step, block_of(direction, step + 1), False).wait_recv()
-
-    def y_all(a):
-        for step in range(half):
-            for direction in range(2 if step < half - 1 else 1):
-                y_arrived(a, direction, step)
+    def y_arrived(a, step):
+        for direction in range(2):
+            for piece in range(2):
+
+                @when((step < half - 1) | (direction == piece))
+                def _():
+                    if over_y(a, piece):
+                        block = block_of(direction, step + 1)
+                        y_copy(a, direction, step, piece, block, False).wait_recv()
+
+    def halo_copy(direction):
+        src = normed.at[pl.ds(tok - 8 if direction == 0 else 0, 8), :]
+        dst = normed.at[pl.ds(tok + 8 * direction, 8), :]
+        return remote(src, dst, halo_s.at[direction], halo_r.at[direction], z_device(direction))
+
+    for direction in range(2):
+        halo_copy(direction).start()
+    if half >= 8:
+        vd_serve(half)
+    for step in range(half):
+        y_arrived(0, step)
+    for direction in range(2):
+        halo_copy(direction).wait_recv()
 
     m_rows = min(256, tok)
     m_count = tok // m_rows
 
-    def up(a, i):
-        rows = pl.ds(pl.multiple_of(i * m_rows, m_rows), m_rows)
+    def put_up(a, made, i):
+        made = made.astype(BF16).astype(F32)
+        ups[a, pl.ds(8 + i * m_rows, m_rows), :] = made[:m_rows]
+        if i == m_count - 1:
+            ups[a, pl.ds(0, 8), :] = jnp.where(s == 0, 0.0, made[m_rows : m_rows + 8])
+            ups[a, pl.ds(tok + 8, 8), :] = jnp.where(s == n_sp - 1, 0.0, made[m_rows + 8 :])
+
+    def up_rows(i):
+        return pl.ds(i * m_rows, m_rows + (16 if i == m_count - 1 else 0))
+
+    for i in range(m_count):
         made = lax.dot_general(
-            normed[rows, :], wbuf[a], (((1,), (1,)), ((), ())), preferred_element_type=F32
+            normed[up_rows(i), :],
+            wbuf[0],
+            (((1,), (1,)), ((), ())),
+            preferred_element_type=F32,
         )
-        ups[a, pl.ds(pl.multiple_of(8 + i * m_rows, 8), m_rows), :] = made.astype(BF16).astype(F32)
-
-    y_all(0)
-
-    @pl.loop(0, m_count)
-    def _(i):
-        up(0, i)
-
-    for k in range(8, half + 1):
-        vd_serve(k)
-    done = min(max(half, 7) - 2, half)
-    y_all(1)
-
-    @pl.loop(0, m_count)
-    def _(i):
-        up(1, i)
-
-        @pl.when(done + 1 + i <= half)
-        def _():
-            w_serve((2,), done + 1 + i)
-
-    done = min(done + m_count, half)
-
-    def halo_copy(direction):
-        if direction == 0:
-            src, dst = ups.at[:, pl.ds(tok, 8), :], ups.at[:, pl.ds(0, 8), :]
-        else:
-            src, dst = ups.at[:, pl.ds(8, 8), :], ups.at[:, pl.ds(tok + 8, 8), :]
-        return remote(src, dst, halo_s.at[direction], halo_r.at[direction], z_device(direction))
-
-    for direction in range(2):
-        halo_copy(direction).start()
+        put_up(0, made, i)
+
+    done = half - 2 if half >= 8 else half
+    w_serve((2,), done + 1)
 
     c_rows = min(32, own)
 
@@ -597,40 +607,61 @@
         start = ((to % 2) * n_x + to // 2) * own + row % own
         return pl.ds(pl.multiple_of(start, c_rows), c_rows)
 
-    c_count = tok // c_rows
-    every = max(c_count // 4, 1)
-
-    @pl.loop(0, c_count)
+    def convolved(a, taps, row):
+        near = ups[a, pl.ds(pl.multiple_of(row, c_rows), c_rows + 16), :]
+        return (
+            taps[0:1, :] * near[7 : 7 + c_rows]
+            + taps[1:2, :] * near[8 : 8 + c_rows]
+            + taps[2:3, :] * near[9 : 9 + c_rows]
+        )
+
+    def blocks(j):
+        return (s + n_sp - j) % n_sp, (s + j % half) % n_sp
+
+    def cols(block):
+        return pl.ds(pl.multiple_of(block * LANES, LANES), LANES)
+
+    def up_value(j, fresh=False, last=False):
+        pair = blocks(j)
+        weights = jnp.concatenate([wbuf[1, :, cols(b)] for b in pair], axis=1)
+        for i in range(m_count):
+            tokens = jnp.concatenate([normed[up_rows(i), cols(b)] for b in pair], axis=1)
+            made = lax.dot_general(
+                tokens, weights, (((1,), (1,)), ((), ())), preferred_element_type=F32
+            )
+            if not fresh:
+                made += partial_up[up_rows(i), :]
+            if last:
+                put_up(1, made, i)
+            else:
+                partial_up[up_rows(i), :] = made
+
+    if half > 1:
+        y_arrived(1, 0)
+        up_value(1, fresh=True)
+
+        @pl.loop(2, half)
+        def _(j):
+            y_arrived(1, j - 1)
+            up_value(j)
+
+    w_serve((2,), done + 2)
+    y_arrived(1, half - 1)
+    up_value(half, last=True)
+    done += 2
+
+    @pl.loop(0, tok // c_rows)
     def _(i):
-        at = (i + 1) % c_count
-
-        @pl.when(i == c_count - 2)
-        def _():
-            for direction in range(2):
-                halo_copy(direction).wait_recv()
-            ups[:, pl.ds(0, 8), :] = jnp.where(s == 0, 0.0, ups[:, pl.ds(0, 8), :])
-            ups[:, pl.ds(tok + 8, 8), :] = jnp.where(
-                s == n_sp - 1, 0.0, ups[:, pl.ds(tok + 8, 8), :]
-            )
-
-        mixed = []
-        for a, taps in ((0, cg_ref), (1, cv_ref)):
-            near = ups[a, pl.ds(pl.multiple_of(at * c_rows, c_rows), c_rows + 16), :]
-            mixed.append(
-                taps[0:1, :] * near[7 : 7 + c_rows]
-                + taps[1:2, :] * near[8 : 8 + c_rows]
-                + taps[2:3, :] * near[9 : 9 + c_rows]
-            )
-        v = mixed[0]
+        row = i * c_rows
+        v = convolved(0, cg_ref, row)
         inner = (2.0 / np.pi) ** 0.5 * (v + 0.044715 * (v * v * v))
-        gated = 0.5 * v * (1.0 + jnp.tanh(inner)) * mixed[1]
-        hidden[by_core(at * c_rows), :] = gated.astype(BF16)
-
-        @pl.when((i % every == every - 1) & (done + 1 + i // every <= half))
-        def _():
-            w_serve((2,), done + 1 + i // every)
-
-    done = min(half, done + c_count // every)
+        gated[pl.ds(pl.multiple_of(row, c_rows), c_rows), :] = 0.5 * v * (1.0 + jnp.tanh(inner))
+
+    @pl.loop(0, tok // c_rows)
+    def _(i):
+        row = i * c_rows
+        gate = gated[pl.ds(pl.multiple_of(row, c_rows), c_rows), :]
+        hidden[by_core(row), :] = (gate * convolved(1, cv_ref, row)).astype(BF16)
 
     per_core = n_x * own
     cut = own // 2
@@ -683,10 +714,9 @@
     def of_chip(chip, size, lo=0):
         return pl.ds(pl.multiple_of(chip * own + lo, 16), size)
 
-    def blocks(j):
-        return (s + n_sp - j) % n_sp, (s + j % half) % n_sp
-
-    @pl.loop(1, half + 3)
+    sum_lag, send_lag = 2, 4
+
+    @pl.loop(1, half + send_lag + 1)
     def _(j):
         @pl.when(j <= half)
         def _():
@@ -694,16 +724,8 @@
             def _():
                 w_serve((2,), j)
 
-            y_arrived(2, 0, j - 1)
-
-            @pl.when(j < half)
-            def _():
-                y_arrived(2, 1, j - 1)
-
+            y_arrived(2, j - 1)
             first, second = blocks(j)
-
-            def cols(block):
-                return pl.ds(pl.multiple_of(block * LANES, LANES), LANES)
 
             @pl.loop(0, m_count)
             def _(i):
@@ -713,13 +735,14 @@
                 part[first, rows, :] = made[:, :LANES]
                 part[second, rows, :] = made[:, LANES:]
 
+
             for i, block in enumerate((first, second)):
                 pair_copy(2 * (j - 1) + i, block, 1 - c).start()
 
-        @pl.when((j >= 2) & (j <= half + 1))
+        @pl.when((j > sum_lag) & (j <= half + sum_lag))
         def _():
-            for i, block in enumerate(blocks(j - 1)):
-                pair_copy(2 * (j - 2) + i, block, c).wait_recv()
+            for i, block in enumerate(blocks(j - sum_lag)):
+                pair_copy(2 * (j - sum_lag - 1) + i, block, c).wait_recv()
                 for chip in (chip_far, chip_right, chip_left):
                     pair_sum[block, of_chip(chip, own), :] = (
                         part[block, of_core(chip, own), :].astype(F32)
@@ -728,9 +751,9 @@
                 for direction in range(2):
                     far_copy(direction, block).start()
 
-        @pl.when(j >= 3)
+        @pl.when(j > send_lag)
         def _():
-            for block in blocks(j - 2):
+            for block in blocks(j - send_lag):
                 for direction in range(2):
                     far_copy(direction, block).wait_recv()
                     chip = chip_right if direction == 0 else chip_left
@@ -776,16 +799,14 @@
                 block = block_of(direction, step)
                 kv_copy(direction, step, piece, block).wait_send()
                 sib_copy(c, direction, step, piece, block_of(direction, step + 1)).wait_send()
+                arriving = block_of(direction, step + 1)
                 if piece == 0:
-                    arriving = block_of(direction, step + 1)
                     xp_copy(direction, step, arriving, True).wait_send()
                     rel_copy(c, direction, step, arriving).wait_send()
                 for a in range(3):
                     w_copy(a, direction, step, piece, block, first=step == 0).wait_send()
-                    if piece == 0:
-                        y_copy(
-                            a, direction, step, block_of(direction, step + 1), True
-                        ).wait_send()
+                    if over_y(a, piece):
+                        y_copy(a, direction, step, piece, arriving, True).wait_send()
 
 
 def body(
@@ -846,9 +867,11 @@
             pltpu.VMEM((n_tp * out_weight.shape[0], model), BF16),
             pltpu.VMEM((own, model), F32),
             pltpu.VMEM((own, model), BF16),
-            pltpu.VMEM((tok, model), BF16),
+            pltpu.VMEM((tok + 16, model), BF16),
             pltpu.VMEM((3, units, model), BF16),
             pltpu.VMEM((2, tok + 16, units), F32),
+            pltpu.VMEM((tok + 16, units), F32),
+            pltpu.VMEM((tok, units), F32),
             pltpu.VMEM((tok, units), BF16),
             pltpu.VMEM((n_sp, tok, LANES), BF16),
             pltpu.VMEM((n_sp, tok // 2, LANES), BF16),
@@ -865,10 +888,10 @@
             dma((2 * half,)),
             dma((12 * half,)),
             dma((12 * half,)),
-            dma((6 * half,)),
-            dma((6 * half,)),
-            dma((19,)),
-            dma((19,)),
+            dma((12 * half,)),
+            dma((12 * half,)),
+            dma((4 * (out_weight.shape[0] // 16) + 3,)),
+            dma((4 * (out_weight.shape[0] // 16) + 3,)),
             dma((9,)),
             dma((9,)),
             dma((n_tp - 1,)),

time: 158 us -> 151 us (0.956)
  Pallas kernels: 156 us -> 149 us
    pallas_call x1, Pallas kernels: 156 us -> 149 us  [body(): pl.pallas_call(functools.partial(ring_kernel, n_sp, n_tp), out_shape=jax....]
where the time goes in v3:
time: 151 us
  Pallas kernels  149 us (99%)
  local copies, waits for them, and re-layouts  1.77 us (1%)
    pallas_call x1, Pallas kernels, body(): pl.pallas_call(functools.partial(ring_kernel, n_sp, n_tp), out_shape=jax....  149 us

profile of v3, /device:TPU:33, one launch (start us, length us, event | category | flops | bytes accessed | tf_op | source)
XLA Modules:
  0.0 150.8 jit_solution(11003540395785867282)
XLA Ops:
  0.0 149.0 %layer.1 = bf16[96,2048]{1,0:T(8,128)(2,1)} custom-call(f32[2,192,128]{2,1,0:T(8,128)} %constant.4.clone.row_tab, f32[2,64,128]{2,1,0:T(8,128)} %constant.5.clone.col_tab, bf16[768,128]{1,0:T(8,128)(2,1)} %q_ref.1, bf16[768,256]{1,0:T(8,128)(2,1)} %k_ref.1, bf16[768,256]{1,0:T(8,128)(2,1)} %v_ref.1, f32[1,128]{1,0:T(1,128)} %bitcast.12, f32[1,128]{1,0:T(1,128)} %bitcast.13, ...), custom_call_target="tpu_custom_call" | custom-call | tf_op jit(solution)/shard_map/layer/pallas_call | solution.py:854
  149.0 1.8 %copy.18 = bf16[96,2048]{1,0:T(8,128)(2,1)} copy(bf16[96,2048]{1,0:T(8,128)(2,1)} %layer.1) | data formatting | bytes 786432

commit v4 on v3

--- a/solution.py
+++ b/solution.py
@@ -71,7 +71,6 @@
     wbuf,
     ups,
     partial_up,
-    gated,
     hidden,
     part,
     pair_in,
@@ -84,8 +83,6 @@
     sib_r,
     xp_s,
     xp_r,
-    rel_s,
-    rel_r,
     w_s,
     w_r,
     y_s,
@@ -162,22 +159,27 @@
     def kv_copy(direction, step, piece, block):
         ref = kv_at(c, block, piece, x % 2)
         i = (direction * half + step) * 2 + piece
-        return remote(ref, ref, kv_s.at[i], kv_r.at[i], z_device(direction))
+        return remote(ref, ref, kv_s, kv_r.at[i], z_device(direction))
 
     def sib_copy(which, direction, step, piece, block):
         ref = kv_at(which, block, piece, x % 2)
-        i = (direction * half + step) * 2 + piece
-        return remote(ref, ref, sib_s.at[i], sib_r.at[i], {"tp": sibling})
+        i = jnp.where(step == half - 1, 0, direction) * half + step
+        return remote(ref, ref, sib_s, sib_r.at[i], {"tp": sibling})
 
     def xp_copy(direction, step, block, mine):
         ref = kv_at(c, block, 0, x % 2 if mine else 1 - x % 2)
         i = direction * half + step
-        return remote(ref, ref, xp_s.at[i], xp_r.at[i], {"tp": 2 * x_pair + c})
+        return remote(ref, ref, xp_s, xp_r.at[i], {"tp": 2 * x_pair + c})
 
     def rel_copy(which, direction, step, block):
         ref = kv_at(which, block, 0, 1 - x % 2)
         i = direction * half + step
-        return remote(ref, ref, rel_s.at[i], rel_r.at[i], {"tp": sibling})
+        return remote(ref, ref, sib_s, sib_r.at[i], {"tp": sibling})
+
+    def sib_block(which, direction, step, block):
+        ref = kv.at[which, pl.ds(pl.multiple_of(block * tok, tok), tok), :]
+        i = direction * half + step
+        return remote(ref, ref, sib_s, sib_r.at[i], {"tp": sibling})
 
     def w_rows(a, piece, side):
         if a == 0:
@@ -199,12 +201,12 @@
         dst = w_at(a, block, rows)
         src = sources[a].at[rows, :] if first else dst
         i = ((a * 2 + direction) * half + step) * 2 + piece
-        return remote(src, dst, w_s.at[i], w_r.at[i], z_device(direction))
+        return remote(src, dst, w_s.at[a], w_r.at[i], z_device(direction))
 
     def y_copy(a, direction, step, piece, block, mine):
         ref = w_at(a, block, w_rows(a, piece, g % 2 if mine else 1 - g % 2))
-        i = ((a * 2 + direction) * half + step) * 2 + piece
-        return remote(ref, ref, y_s.at[i], y_r.at[i], {"grp": partner})
+        i = 0 if a == 0 else 1 + (a - 1) * half + step
+        return remote(ref, ref, y_s.at[a], y_r.at[i], {"grp": partner})
 
     def w_start(arrays):
         for piece in range(2):
@@ -245,12 +247,12 @@
             dst = at(2 * chip + c, lo, size)
             i = direction * 2 + step
             device = {"tp": x_right if direction == 0 else x_left}
-            return remote(dst if src is None else src, dst, send.at[i], recv.at[i], device)
-
-        def share(i, chip, core, lo, size, src=None):
+            return remote(dst if src is None else src, dst, send, recv.at[i], device)
+
+        def share(chip, core, lo, size, src=None):
             dst = at(2 * chip + core, lo, size)
             return remote(
-                dst if src is None else src, dst, send.at[4 + i], recv.at[4 + i], {"tp": sibling}
+                dst if src is None else src, dst, send, recv.at[4], {"tp": sibling}
             )
 
         chips = ((x + n_x - 1) % n_x, (x + 1) % n_x)
@@ -259,34 +261,29 @@
         def start():
             for direction in range(2):
                 ring(direction, 0, x, 0, rows, first).start()
-            share(4, x, c, 0, rows, first).start()
+            share(x, c, 0, rows, first).start()
 
         def middle():
             for direction in range(2):
                 chip = chips[direction]
                 ring(direction, 0, chip, 0, rows).wait_recv()
                 ring(direction, 1, chip, direction * hold, hold).start()
-                share(direction, chip, c, 0, rows).start()
+                share(chip, c, 0, rows).start()
 
         def end():
             for direction in range(2):
                 ring(direction, 1, far, direction * hold, hold).wait_recv()
-                share(2 + direction, far, c, direction * hold, hold).start()
+                share(far, c, direction * hold, hold).start()
+
+        def all_rows(blocks):
+            ref = buf.at[pl.ds(0, blocks * rows), :]
+            return remote(ref, ref, send, recv.at[4], {"tp": sibling})
 
         def arrived():
-            other = 1 - c
-            share(4, x, other, 0, rows).wait_recv()
-            for direction in range(2):
-                share(direction, chips[direction], other, 0, rows).wait_recv()
-                share(2 + direction, far, other, direction * hold, hold).wait_recv()
+            all_rows(n_x).wait_recv()
 
         def sent():
-            for direction in range(2):
-                ring(direction, 0, x, 0, rows, first).wait_send()
-                ring(direction, 1, chips[direction], direction * hold, hold).wait_send()
-                share(direction, chips[direction], c, 0, rows).wait_send()
-                share(2 + direction, far, c, direction * hold, hold).wait_send()
-            share(4, x, c, 0, rows, first).wait_send()
+            all_rows(2 * n_x - 1).wait_send()
 
         return start, middle, end, arrived, sent
 
@@ -297,7 +294,7 @@
     def ow_copy(i, chip, core, lo, size, device, first=False):
         dst = ow_all.at[pl.ds(pl.multiple_of((2 * chip + core) * ow_rows + lo, 16), size), :]
         src = ow_ref.at[pl.ds(lo, size), :] if first else dst
-        return remote(src, dst, ow_s.at[i], ow_r.at[i], {"tp": device})
+        return remote(src, dst, ow_s, ow_r.at[i], {"tp": device})
 
     size = ow_rows // ow_parts
 
@@ -314,7 +311,7 @@
         return ow_copy(2 * ow_parts + 1, x, core, 0, ow_rows, sibling, first)
 
     def ow_share(i, chip, core, lo, size):
-        return ow_copy(2 * ow_parts + 2 + i, chip, core, lo, size, sibling)
+        return ow_copy(2 * ow_parts + 1, chip, core, lo, size, sibling)
 
     def ow_shares(core, i):
         if i == ow_parts:
@@ -322,6 +319,10 @@
         if i < ow_parts:
             return ow_share(i, x_pair, core, i * size, size)
         return ow_share(i, ow_far, core, (i - ow_parts - 1) * size, size)
+
+    def ow_bytes(blocks):
+        ref = ow_all.at[pl.ds(0, blocks * ow_rows), :]
+        return remote(ref, ref, ow_s, ow_r.at[2 * ow_parts + 1], {"tp": sibling})
 
     def ow_take(q):
         ow_pair(q, x_pair).wait_recv()
@@ -449,16 +450,10 @@
 
         for direction in range(2):
             block = block_of(direction, k - 2)
-            for piece in range(2):
-                last = direction == piece
-
-                @pl.when((k >= 3) & (k <= half + 2 if last else k <= half + 1))
-                def _():
-                    sib_copy(1 - c, direction, k - 3, piece, block).wait_recv()
 
             @pl.when((k >= 3) & (k <= half + 2 if direction == 0 else k <= half + 1))
             def _():
-                rel_copy(1 - c, direction, k - 3, block).wait_recv()
+                sib_block(1 - c, direction, k - 3, block).wait_recv()
 
         @pl.when(k != 2)
         def _():
@@ -479,39 +474,42 @@
 
         at_step(half + 2, lambda: w_serve((1,), 1))
 
+    d_lag = 2
+
     def vd_serve(k):
         for piece in range(2):
             w_serve((1,), k, (piece,))
-            w_serve((2,), k - 2, (piece,))
-        if k == 2:
+            w_serve((2,), k - d_lag, (piece,))
+        if k == d_lag:
             w_start((2,))
 
     att_own[...] = (acc[...] / den[...]).astype(BF16)
 
-    def att_copy(i, to, source):
+    def att_copy(to, source):
         cols = pl.ds(pl.multiple_of(source * LANES, LANES), LANES)
         rows = pl.ds(pl.multiple_of(to * own, 16), own)
         return remote(
             att_own.at[rows, :],
             att_all.at[:, cols],
-            a2a_s.at[i - 1],
-            a2a_r.at[i - 1],
+            a2a_s,
+            a2a_r,
             {"tp": to},
         )
 
     for i in range(1, n_tp):
-        att_copy(i, (t + i) % n_tp, t).start()
+        att_copy((t + i) % n_tp, t).start()
     att_all[:, pl.ds(pl.multiple_of(t * LANES, LANES), LANES)] = att_own[
         pl.ds(pl.multiple_of(t * own, 16), own), :
     ]
     vd_serve(2)
     for q in range(ow_in_loop, ow_parts):
         ow_take_far(q)
-    for i in range(2 * ow_parts + 1):
-        ow_shares(1 - c, i).wait_recv()
-    ow_own(1 - c).wait_recv()
-    for i in range(1, n_tp):
-        att_copy(i, t, (t + n_tp - i) % n_tp).wait_recv()
+    ow_bytes(n_x).wait_recv()
+    def att_bytes():
+        ref = att_all.at[:, pl.ds(0, (n_tp - 1) * LANES)]
+        return remote(ref, ref, a2a_s, a2a_r, {"tp": sibling})
+
+    att_bytes().wait_recv()
 
     width = min(512, model)
 
@@ -551,29 +549,36 @@
     vd_serve(7)
     nm_arrived()
 
+    def w_bytes(a, rows, blocks, send, recv):
+        ref = wbuf.at[a, pl.ds(0, rows), pl.ds(0, blocks * LANES)]
+        return remote(ref, ref, send, recv, {"grp": partner})
+
     def y_arrived(a, step):
-        for direction in range(2):
-            for piece in range(2):
-
-                @when((step < half - 1) | (direction == piece))
-                def _():
-                    if over_y(a, piece):
-                        block = block_of(direction, step + 1)
-                        y_copy(a, direction, step, piece, block, False).wait_recv()
+        if a == 0:
+            w_bytes(0, units // 2, n_sp - 1, y_s.at[0], y_r.at[0]).wait_recv()
+            return
+        i = 1 + (a - 1) * half + step
+        for last, count in ((False, 2), (True, 1)):
+
+            @when((step == half - 1) == last)
+            def _():
+                w_bytes(a, private, count, y_s.at[a], y_r.at[i]).wait_recv()
 
     def halo_copy(direction):
         src = normed.at[pl.ds(tok - 8 if direction == 0 else 0, 8), :]
         dst = normed.at[pl.ds(tok + 8 * direction, 8), :]
-        return remote(src, dst, halo_s.at[direction], halo_r.at[direction], z_device(direction))
+        return remote(src, dst, halo_s, halo_r, z_device(direction))
 
     for direction in range(2):
         halo_copy(direction).start()
     if half >= 8:
         vd_serve(half)
-    for step in range(half):
-        y_arrived(0, step)
-    for direction in range(2):
-        halo_copy(direction).wait_recv()
+    y_arrived(0, None)
+    def halo_bytes():
+        ref = normed.at[pl.ds(tok, 16), :]
+        return remote(ref, ref, halo_s, halo_r, z_device(0))
+
+    halo_bytes().wait_recv()
 
     m_rows = min(256, tok)
     m_count = tok // m_rows
@@ -597,18 +602,13 @@
         )
         put_up(0, made, i)
 
-    done = half - 2 if half >= 8 else half
+    done = half - d_lag if half >= 8 else half
     w_serve((2,), done + 1)
 
-    c_rows = min(32, own)
-
-    def by_core(row):
-        to = row // own
-        start = ((to % 2) * n_x + to // 2) * own + row % own
-        return pl.ds(pl.multiple_of(start, c_rows), c_rows)
+    c_rows = own // 2
 
     def convolved(a, taps, row):
-        near = ups[a, pl.ds(pl.multiple_of(row, c_rows), c_rows + 16), :]
+        near = ups[a, pl.ds(pl.multiple_of(row, 8), c_rows + 16), :]
         return (
             taps[0:1, :] * near[7 : 7 + c_rows]
             + taps[1:2, :] * near[8 : 8 + c_rows]
@@ -645,76 +645,68 @@
             y_arrived(1, j - 1)
             up_value(j)
 
-    w_serve((2,), done + 2)
+            @pl.when(j == half // 2)
+            def _():
+                w_serve((2,), done + 2)
+
+    w_serve((2,), done + 3)
     y_arrived(1, half - 1)
     up_value(half, last=True)
-    done += 2
-
-    @pl.loop(0, tok // c_rows)
+    done = min(done + 3, half) if half > 2 else half
+
+    @pl.loop(0, 2 * n_tp)
     def _(i):
-        row = i * c_rows
-        v = convolved(0, cg_ref, row)
+        to, lower = i // 2, i % 2
+        v = convolved(0, cg_ref, i * c_rows)
         inner = (2.0 / np.pi) ** 0.5 * (v + 0.044715 * (v * v * v))
-        gated[pl.ds(pl.multiple_of(row, c_rows), c_rows), :] = 0.5 * v * (1.0 + jnp.tanh(inner))
-
-    @pl.loop(0, tok // c_rows)
-    def _(i):
-        row = i * c_rows
-        gate = gated[pl.ds(pl.multiple_of(row, c_rows), c_rows), :]
-        hidden[by_core(row), :] = (gate * convolved(1, cv_ref, row)).astype(BF16)
+        gated = 0.5 * v * (1.0 + jnp.tanh(inner)) * convolved(1, cv_ref, i * c_rows)
+        start = ((to % 2) * n_x + to // 2) * own + lower * c_rows
+        hidden[pl.ds(pl.multiple_of(start, 8), c_rows), :] = gated.astype(BF16)
 
     per_core = n_x * own
-    cut = own // 2
-    chip_right, chip_left = (x + 1) % n_x, (x + n_x - 1) % n_x
+    chips = ((x + 1) % n_x, (x + n_x - 1) % n_x)
     chip_far = (x + 2) % n_x
-
-    def pair_copy(i, block, core):
-        rows = pl.ds(pl.multiple_of(core * per_core, 16), per_core)
+    toward = ({"tp": x_right}, {"tp": x_left})
+
+    def rows_at(start, size):
+        return pl.ds(pl.multiple_of(start, 16), size)
+
+    def pair_copy(j, block, core):
         return remote(
-            part.at[block, rows, :],
+            part.at[block, rows_at(core * per_core, per_core), :],
             pair_in.at[block],
-            pair_s.at[i],
-            pair_r.at[i],
+            pair_s,
+            pair_r.at[j - 1],
             {"tp": sibling},
         )
 
-    def far_copy(direction, block):
-        lo = cut if direction == 0 else 0
+    def far_copy(j, direction, block):
         return remote(
-            pair_sum.at[block, pl.ds(pl.multiple_of(chip_far * own + lo, 16), cut), :],
-            far_in.at[direction, block],
-            far_s.at[direction * n_sp + block],
-            far_r.at[direction * n_sp + block],
-            {"tp": x_right if direction == 0 else x_left},
+            pair_sum.at[block, rows_at(chip_far * own, own), :],
+            far_in.at[block],
+            far_s,
+            far_r.at[j - 1],
+            toward[direction],
         )
 
     def near_copy(direction, block):
-        chip = chip_right if direction == 0 else chip_left
         return remote(
-            pair_sum.at[block, pl.ds(pl.multiple_of(chip * own, 16), own), :],
+            pair_sum.at[block, rows_at(chips[direction] * own, own), :],
             near_in.at[direction, block],
-            near_s.at[direction],
-            near_r.at[direction],
-            {"tp": x_right if direction == 0 else x_left},
+            near_s,
+            near_r,
+            toward[direction],
         )
 
-    def near_all(direction):
-        ref = near_in.at[direction]
-        return remote(
-            ref,
-            ref,
-            near_s.at[direction],
-            near_r.at[direction],
-            {"tp": x_right if direction == 0 else x_left},
-        )
-
-    def of_core(chip, size, lo=0):
-        return pl.ds(pl.multiple_of(c * per_core + chip * own + lo, 16), size)
-
-    def of_chip(chip, size, lo=0):
-        return pl.ds(pl.multiple_of(chip * own + lo, 16), size)
-
-    sum_lag, send_lag = 2, 4
+    def bytes_of(ref, send, recv):
+        return remote(ref, ref, send, recv, {"tp": sibling})
+
+    def pair_added(block, chip):
+        mine = part[block, rows_at(c * per_core + chip * own, own), :]
+        other = pair_in[block, rows_at(chip * own, own), :]
+        return mine.astype(F32) + other.astype(F32)
+
+    sum_lag, send_lag = 1, 3
 
     @pl.loop(1, half + send_lag + 1)
     def _(j):
@@ -726,87 +718,71 @@
 
             y_arrived(2, j - 1)
             first, second = blocks(j)
-
-            @pl.loop(0, m_count)
+            both = jnp.concatenate([wbuf[2, :, cols(first)], wbuf[2, :, cols(second)]], axis=1)
+
+            @pl.loop(0, m_count, unroll=True)
             def _(i):
                 rows = pl.ds(pl.multiple_of(i * m_rows, m_rows), m_rows)
-                both = jnp.concatenate([wbuf[2, :, cols(first)], wbuf[2, :, cols(second)]], axis=1)
                 made = jnp.dot(hidden[rows, :], both, preferred_element_type=F32).astype(BF16)
                 part[first, rows, :] = made[:, :LANES]
                 part[second, rows, :] = made[:, LANES:]
 
-
-            for i, block in enumerate((first, second)):
-                pair_copy(2 * (j - 1) + i, block, 1 - c).start()
+            for block in (first, second):
+                pair_copy(j, block, 1 - c).start()
 
         @pl.when((j > sum_lag) & (j <= half + sum_lag))
         def _():
-            for i, block in enumerate(blocks(j - sum_lag)):
-                pair_copy(2 * (j - sum_lag - 1) + i, block, c).wait_recv()
-                for chip in (chip_far, chip_right, chip_left):
-                    pair_sum[block, of_chip(chip, own), :] = (
-                        part[block, of_core(chip, own), :].astype(F32)
-                        + pair_in[block, of_chip(chip, own), :].astype(F32)
-                    ).astype(BF16)
-                for direction in range(2):
-                    far_copy(direction, block).start()
+            two = pair_in.at[pl.ds(0, 2)]
+            bytes_of(two, pair_s, pair_r.at[j - sum_lag - 1]).wait_recv()
+            for direction, block in enumerate(blocks(j - sum_lag)):
+                for chip in (chip_far, chips[1 - direction]):
+                    pair_sum[block, rows_at(chip * own, own), :] = pair_added(block, chip).astype(
+                        BF16
+                    )
+                far_copy(j - sum_lag, direction, block).start()
+                near_copy(1 - direction, block).start()
 
         @pl.when(j > send_lag)
         def _():
-            for block in blocks(j - send_lag):
-                for direction in range(2):
-                    far_copy(direction, block).wait_recv()
-                    chip = chip_right if direction == 0 else chip_left
-                    lo = cut if direction == 0 else 0
-                    pair_sum[block, of_chip(chip, cut, lo), :] = (
-                        part[block, of_core(chip, cut, lo), :].astype(F32)
-                        + pair_in[block, of_chip(chip, cut, lo), :].astype(F32)
-                        + far_in[direction, block].astype(F32)
-                    ).astype(BF16)
-                    near_copy(direction, block).start()
-
-    for direction in range(2):
-        near_all(direction).wait_recv()
+            two = far_in.at[pl.ds(0, 2)]
+            bytes_of(two, far_s, far_r.at[j - send_lag - 1]).wait_recv()
+            for direction, block in enumerate(blocks(j - send_lag)):
+                chip = chips[direction]
+                pair_sum[block, rows_at(chip * own, own), :] = (
+                    pair_added(block, chip) + far_in[block].astype(F32)
+                ).astype(BF16)
+                near_copy(direction, block).start()
+
+    bytes_of(near_in, near_s, near_r).wait_recv()
 
     for b in range(n_sp):
         span = slice(b * LANES, (b + 1) * LANES)
-        total = part[b, of_core(x, own), :].astype(F32) + pair_in[b, of_chip(x, own), :].astype(F32)
+        total = pair_added(b, x)
         for direction in range(2):
             total += near_in[direction, b].astype(F32)
         out_ref[:, span] = (stream[:, span].astype(F32) + total).astype(BF16)
 
-    for q in range(ow_parts):
-        ow_pair(q, x, first=True).wait_send()
-        ow_on(q, x_pair).wait_send()
-    ow_over(x, first=True).wait_send()
-    for i in range(2 * ow_parts + 1):
-        ow_shares(c, i).wait_send()
-    ow_own(c, first=True).wait_send()
+    ow_bytes(2 * n_x - 1).wait_send()
     nm_sent()
-    for i in range(1, n_tp):
-        att_copy(i, (t + i) % n_tp, t).wait_send()
-    for b in range(n_sp):
-        pair_copy(b, b, 1 - c).wait_send()
-        for direction in range(2):
-            far_copy(direction, b).wait_send()
-    for direction in range(2):
-        near_all(direction).wait_send()
-        halo_copy(direction).wait_send()
-        for step in range(half):
-            for piece in range(2):
-                if step == half - 1 and direction != piece:
-                    continue
-                block = block_of(direction, step)
-                kv_copy(direction, step, piece, block).wait_send()
-                sib_copy(c, direction, step, piece, block_of(direction, step + 1)).wait_send()
-                arriving = block_of(direction, step + 1)
-                if piece == 0:
-                    xp_copy(direction, step, arriving, True).wait_send()
-                    rel_copy(c, direction, step, arriving).wait_send()
-                for a in range(3):
-                    w_copy(a, direction, step, piece, block, first=step == 0).wait_send()
-                    if over_y(a, piece):
-                        y_copy(a, direction, step, piece, arriving, True).wait_send()
+    att_bytes().wait_send()
+    halo_bytes().wait_send()
+    bytes_of(pair_in, pair_s, pair_r.at[0]).wait_send()
+    bytes_of(far_in, far_s, far_r.at[0]).wait_send()
+    bytes_of(near_in, near_s, near_r).wait_send()
+    turns = n_sp - 1
+
+    def kv_bytes(rows, send):
+        ref = kv.at[0, pl.ds(0, rows), :]
+        return remote(ref, ref, send, sib_r.at[0], {"tp": sibling})
+
+    kv_bytes(turns * (kv_private + kv_common), kv_s).wait_send()
+    kv_bytes(turns * kv_private, xp_s).wait_send()
+    kv_bytes(turns * tok, sib_s).wait_send()
+    for a in range(3):
+        along = units // 2 if a == 0 else private + common
+        over = units // 2 if a == 0 else private
+        w_bytes(a, along, turns, w_s.at[a], w_r.at[0]).wait_send()
+        w_bytes(a, over, turns, y_s.at[a], y_r.at[0]).wait_send()
 
 
 def body(
@@ -871,39 +847,36 @@
             pltpu.VMEM((3, units, model), BF16),
             pltpu.VMEM((2, tok + 16, units), F32),
             pltpu.VMEM((tok + 16, units), F32),
-            pltpu.VMEM((tok, units), F32),
             pltpu.VMEM((tok, units), BF16),
             pltpu.VMEM((n_sp, tok, LANES), BF16),
             pltpu.VMEM((n_sp, tok // 2, LANES), BF16),
             pltpu.VMEM((n_sp, tok // 2, LANES), BF16),
-            pltpu.VMEM((2, n_sp, own // 2, LANES), BF16),
+            pltpu.VMEM((n_sp, own, LANES), BF16),
             pltpu.VMEM((2, n_sp, own, LANES), BF16),
+            dma,
             dma((4 * half,)),
-            dma((4 * half,)),
-            dma((4 * half,)),
-            dma((4 * half,)),
+            dma,
             dma((2 * half,)),
+            dma,
             dma((2 * half,)),
-            dma((2 * half,)),
-            dma((2 * half,)),
+            dma((3,)),
             dma((12 * half,)),
-            dma((12 * half,)),
-            dma((12 * half,)),
-            dma((12 * half,)),
-            dma((4 * (out_weight.shape[0] // 16) + 3,)),
-            dma((4 * (out_weight.shape[0] // 16) + 3,)),
-            dma((9,)),
-            dma((9,)),
-            dma((n_tp - 1,)),
-            dma((n_tp - 1,)),
-            dma((2,)),
-            dma((2,)),
-            dma((n_sp,)),
-            dma((n_sp,)),
-            dma((2 * n_sp,)),
-            dma((2 * n_sp,)),
-            dma((2,)),
-            dma((2,)),
+            dma((3,)),
+            dma((2 * half + 1,)),
+            dma,
+            dma((2 * (out_weight.shape[0] // 16) + 2,)),
+            dma,
+            dma((5,)),
+            dma,
+            dma,
+            dma,
+            dma,
+            dma,
+            dma((half,)),
+            dma,
+            dma((half,)),
+            dma,
+            dma,
         ],
         compiler_params=pltpu.CompilerParams(
             collective_id=0,

time: 151 us -> 146 us (0.967)
  Pallas kernels: 149 us -> 144 us
    pallas_call x1, Pallas kernels: 149 us -> 144 us  [body(): pl.pallas_call(functools.partial(ring_kernel, n_sp, n_tp), out_shape=jax....]
where the time goes in v4:
time: 146 us
  Pallas kernels  144 us (99%)
  local copies, waits for them, and re-layouts  1.77 us (1%)
    pallas_call x1, Pallas kernels, body(): pl.pallas_call(functools.partial(ring_kernel, n_sp, n_tp), out_shape=jax....  144 us

profile of v4, /device:TPU:33, one launch (start us, length us, event | category | flops | bytes accessed | tf_op | source)
XLA Modules:
  0.0 145.6 jit_solution(3534075997996700784)
XLA Ops:
  0.0 143.8 %layer.1 = bf16[96,2048]{1,0:T(8,128)(2,1)} custom-call(f32[2,192,128]{2,1,0:T(8,128)} %constant.4.clone.row_tab, f32[2,64,128]{2,1,0:T(8,128)} %constant.5.clone.col_tab, bf16[768,128]{1,0:T(8,128)(2,1)} %q_ref.1, bf16[768,256]{1,0:T(8,128)(2,1)} %k_ref.1, bf16[768,256]{1,0:T(8,128)(2,1)} %v_ref.1, f32[1,128]{1,0:T(1,128)} %bitcast.12, f32[1,128]{1,0:T(1,128)} %bitcast.13, ...), custom_call_target="tpu_custom_call" | custom-call | tf_op jit(solution)/shard_map/layer/pallas_call | solution.py:830
  143.8 1.8 %copy.18 = bf16[96,2048]{1,0:T(8,128)(2,1)} copy(bf16[96,2048]{1,0:T(8,128)(2,1)} %layer.1) | data formatting | bytes 786432

commit v5 on v4

--- a/solution.py
+++ b/solution.py
@@ -571,14 +571,10 @@
 
     for direction in range(2):
         halo_copy(direction).start()
-    if half >= 8:
-        vd_serve(half)
     y_arrived(0, None)
     def halo_bytes():
         ref = normed.at[pl.ds(tok, 16), :]
         return remote(ref, ref, halo_s, halo_r, z_device(0))
-
-    halo_bytes().wait_recv()
 
     m_rows = min(256, tok)
     m_count = tok // m_rows
@@ -594,6 +590,8 @@
         return pl.ds(i * m_rows, m_rows + (16 if i == m_count - 1 else 0))
 
     for i in range(m_count):
+        if i == m_count - 1:
+            halo_bytes().wait_recv()
         made = lax.dot_general(
             normed[up_rows(i), :],
             wbuf[0],
@@ -602,8 +600,9 @@
         )
         put_up(0, made, i)
 
+    if half >= 8:
+        vd_serve(half)
     done = half - d_lag if half >= 8 else half
-    w_serve((2,), done + 1)
 
     c_rows = own // 2
 
@@ -645,14 +644,10 @@
             y_arrived(1, j - 1)
             up_value(j)
 
-            @pl.when(j == half // 2)
-            def _():
-                w_serve((2,), done + 2)
-
-    w_serve((2,), done + 3)
     y_arrived(1, half - 1)
     up_value(half, last=True)
-    done = min(done + 3, half) if half > 2 else half
+    w_serve((2,), done + 1)
+    done = min(done + 1, half)
 
     @pl.loop(0, 2 * n_tp)
     def _(i):
@@ -662,6 +657,9 @@
         gated = 0.5 * v * (1.0 + jnp.tanh(inner)) * convolved(1, cv_ref, i * c_rows)
         start = ((to % 2) * n_x + to // 2) * own + lower * c_rows
         hidden[pl.ds(pl.multiple_of(start, 8), c_rows), :] = gated.astype(BF16)
+
+    w_serve((2,), done + 1)
+    done = min(done + 1, half)
 
     per_core = n_x * own
     chips = ((x + 1) % n_x, (x + n_x - 1) % n_x)

time: 146 us -> 143 us (0.979)
  Pallas kernels: 144 us -> 141 us
    pallas_call x1, Pallas kernels: 144 us -> 141 us  [body(): pl.pallas_call(functools.partial(ring_kernel, n_sp, n_tp), out_shape=jax....]
where the time goes in v5:
time: 143 us
  Pallas kernels  141 us (99%)
  local copies, waits for them, and re-layouts  1.77 us (1%)
    pallas_call x1, Pallas kernels, body(): pl.pallas_call(functools.partial(ring_kernel, n_sp, n_tp), out_shape=jax....  141 us

profile of v5, /device:TPU:33, one launch (start us, length us, event | category | flops | bytes accessed | tf_op | source)
XLA Modules:
  0.0 143.3 jit_solution(11631049334347460588)
XLA Ops:
  0.0 141.5 %layer.1 = bf16[96,2048]{1,0:T(8,128)(2,1)} custom-call(f32[2,192,128]{2,1,0:T(8,128)} %constant.4.clone.row_tab, f32[2,64,128]{2,1,0:T(8,128)} %constant.5.clone.col_tab, bf16[768,128]{1,0:T(8,128)(2,1)} %q_ref.1, bf16[768,256]{1,0:T(8,128)(2,1)} %k_ref.1, bf16[768,256]{1,0:T(8,128)(2,1)} %v_ref.1, f32[1,128]{1,0:T(1,128)} %bitcast.12, f32[1,128]{1,0:T(1,128)} %bitcast.13, ...), custom_call_target="tpu_custom_call" | custom-call | tf_op jit(solution)/shard_map/layer/pallas_call | solution.py:828
  141.5 1.8 %copy.18 = bf16[96,2048]{1,0:T(8,128)(2,1)} copy(bf16[96,2048]{1,0:T(8,128)(2,1)} %layer.1) | data formatting | bytes 786432
